TPU v7x, 32 devices: a whole 2x2x4 slice. The times are simulated.
32 devices in a mesh: sp: 8 (over z, y), tp: 4 (over x, core).
Axes of the slice: x: 2, y: 2, z: 4, core: 2. Of those that a mesh axis runs over, the one named last changes fastest.
Arguments:
- tokens_in: bfloat16 [2048, 2048], P('sp'), may hold values from -3 to 3
- queries: bfloat16 [2048, 1024], P('sp', 'tp'), may hold values from -6 to 6
- keys: bfloat16 [2048, 256], P('sp', 'tp'), may hold values from -6 to 6
- values: bfloat16 [2048, 256], P('sp', 'tp'), may hold values from -12 to 12
- doc_ids: int32 [2048], P('sp'), may hold values from 0 to 1, never falling along the last dimension, each value on 1 to 1280 neighbouring positions
- query_gain: float32 [64], replicated, may hold values from 2.5 to 6
- key_norm_scale: float32 [64], replicated, may hold values from 2.5 to 6
- out_weight: bfloat16 [1024, 2048], P('tp'), may hold values from -0.1875 to 0.1875
- norm_gain: float32 [2048], replicated, may hold values from 0.1 to 1.9
- gate_weight: bfloat16 [2048, 5632], P('sp', 'tp'), may hold values from -0.125 to 0.125
- up_weight: bfloat16 [2048, 5632], P('sp', 'tp'), may hold values from -0.125 to 0.125
- down_weight: bfloat16 [5632, 2048], P('tp', 'sp'), may hold values from -0.078125 to 0.078125
Outputs:
- layer_out: bfloat16 [2048, 2048], P('sp')
Inputs may be any that keep to these rules, and one draw needn't show every extreme that they name: `doc_ids`: document numbers never fall along the sequence; every document has 1 to 1280 positions and one has exactly 1280.
All inputs are finite; a program needn't handle non-finite values.
Results may differ from a plain program's by a relative error of at most 0.014.
The roundings to bfloat16 on the way count: a program that leaves them out, or rounds other values in their place, can miss the bound.
Values may be sent and summed in bfloat16 or wider, within the bound.
A program may use at most 128 MiB of HBM per device.

v0:
```python
import functools

import jax
import jax.numpy as jnp
from jax import lax
from jax.experimental import pallas as pl
from jax.experimental.pallas import tpu as pltpu
from jax.sharding import PartitionSpec as P

GRID = 64


EPS = 1e-06
THETA = 10000.0
NEG = -1e30


def rotate_half(block, angle):
    half_dim = block.shape[-1] // 2
    cosine = jnp.cos(angle)[:, None, :]
    sine = jnp.sin(angle)[:, None, :]
    first = block[..., :half_dim]
    second = block[..., half_dim:]
    return jnp.concatenate(
        [first * cosine - second * sine, second * cosine + first * sine], axis=-1
    )


def normalized_rotated(values_in, gain, heads, lattice_row, lattice_column):
    full = values_in.astype(jnp.float32).reshape(values_in.shape[0], heads, -1)
    full = full * lax.rsqrt(jnp.mean(full * full, axis=-1, keepdims=True) + EPS) * gain
    half_dim = full.shape[-1] // 2
    freqs = THETA ** (-2.0 * jnp.arange(half_dim // 2, dtype=jnp.float32) / half_dim)
    by_row = rotate_half(full[..., :half_dim], lattice_row[:, None] * freqs[None, :])
    by_col = rotate_half(full[..., half_dim:], lattice_column[:, None] * freqs[None, :])
    return jnp.concatenate([by_row, by_col], axis=-1).astype(jnp.bfloat16)


MESH = pl.DeviceIdType.MESH
VM = pl.BlockSpec(memory_space=pltpu.VMEM)


def params(cid):
    return pltpu.CompilerParams(
        collective_id=cid, has_side_effects=True, vmem_limit_bytes=56 * 1024 * 1024
    )


def greet(count, where):
    barrier = pltpu.get_barrier_semaphore()

    @pl.loop(1, count)
    def _(step):
        pl.semaphore_signal(barrier, inc=1, device_id=where(step), device_id_type=MESH)

    pl.semaphore_wait(barrier, count - 1)


def gather_kernel(n, kv_ref, doc_ref, kv_out, doc_out, send, recv, doc_send, doc_recv):
    me = lax.axis_index("sp")

    def where(step):
        return {"sp": lax.rem(me + step, n)}

    def copies(step, slot):
        return (
            pltpu.make_async_remote_copy(
                kv_ref, kv_out.at[slot], send.at[step], recv.at[step], where(step), MESH
            ),
            pltpu.make_async_remote_copy(
                doc_ref, doc_out.at[slot], doc_send.at[step], doc_recv.at[step], where(step), MESH
            ),
        )

    greet(n, where)

    @pl.loop(1, n)
    def _(step):
        for copy in copies(step, me):
            copy.start()

    kv_out[me] = kv_ref[...]
    doc_out[me] = doc_ref[...]

    @pl.loop(1, n)
    def _(step):
        for copy in copies(step, lax.rem(me + n - step, n)):
            copy.wait_recv()
            copy.wait_send()


def gather_sp(n, packed, docs):
    return pl.pallas_call(
        functools.partial(gather_kernel, n),
        out_shape=(
            jax.ShapeDtypeStruct((n,) + packed.shape, packed.dtype),
            jax.ShapeDtypeStruct((n,) + docs.shape, docs.dtype),
        ),
        in_specs=[VM, VM],
        out_specs=(VM, VM),
        scratch_shapes=[pltpu.SemaphoreType.DMA((n,))] * 4,
        compiler_params=params(0),
        name="gather_sp",
    )(packed, docs)


def mid_kernel(
    nt, partial_ref, tokens_ref, gain_ref, normed_out, resid_out, landing, send, recv, send2, recv2
):
    sp, tp = lax.axis_index("sp"), lax.axis_index("tp")
    side = lax.rem(sp, 2)
    base = sp - side
    group = 2 * nt
    me = side * nt + tp
    rows = resid_out.shape[0]

    def where(step):
        other = lax.rem(me + step, group)
        return {"sp": base + other // nt, "tp": lax.rem(other, nt)}

    def part(step):
        peer = lax.rem(tp + step, nt)
        return pltpu.make_async_remote_copy(
            partial_ref.at[peer],
            landing.at[step],
            send.at[step],
            recv.at[step],
            {"sp": sp, "tp": peer},
            MESH,
        )

    def spread(step, slot):
        return pltpu.make_async_remote_copy(
            normed_out.at[slot], normed_out.at[slot], send2.at[step], recv2.at[step], where(step), MESH
        )

    greet(group, where)
    for step in range(1, nt):
        part(step).start()
    for step in range(1, nt):
        part(step).wait_recv()
    chunk = 16

    @pl.loop(0, rows // chunk)
    def _(i):
        at = pl.ds(pl.multiple_of(i * chunk, chunk), chunk)
        mixed = partial_ref[tp, at].astype(jnp.float32)
        for step in range(1, nt):
            mixed = mixed + landing[step, at].astype(jnp.float32)
        resid = tokens_ref[tp, at].astype(jnp.float32) + mixed
        resid_out[at] = resid
        power = jnp.mean(resid * resid, axis=-1, keepdims=True)
        normed_out[me, at] = (resid * lax.rsqrt(power + EPS) * gain_ref[...]).astype(jnp.bfloat16)

    for step in range(1, group):
        spread(step, me).start()
    for step in range(1, group):
        copy = spread(step, lax.rem(me + group - step, group))
        copy.wait_recv()
        copy.wait_send()
    for step in range(1, nt):
        part(step).wait_send()


def mid_stage(nt, part, tokens, gain):
    rows, width = part.shape[0] // nt, part.shape[1]
    return pl.pallas_call(
        functools.partial(mid_kernel, nt),
        out_shape=(
            jax.ShapeDtypeStruct((2 * nt, rows, width), jnp.bfloat16),
            jax.ShapeDtypeStruct((rows, width), jnp.float32),
        ),
        in_specs=[VM, VM, VM],
        out_specs=(VM, VM),
        scratch_shapes=[pltpu.VMEM((nt, rows, width), jnp.bfloat16)]
        + [pltpu.SemaphoreType.DMA((nt,))] * 2
        + [pltpu.SemaphoreType.DMA((2 * nt,))] * 2,
        compiler_params=params(1),
        name="mid_stage",
    )(part.reshape(nt, rows, width), tokens.reshape(nt, rows, width), gain.reshape(1, width))


def last_kernel(nt, fed_ref, resid_ref, out_ref, landing, send, recv, send2, recv2):
    sp, tp = lax.axis_index("sp"), lax.axis_index("tp")
    side = lax.rem(sp, 2)
    base = sp - side
    group = 2 * nt
    me = side * nt + tp
    rows = resid_ref.shape[0]

    def where(step):
        other = lax.rem(me + step, group)
        return {"sp": base + other // nt, "tp": lax.rem(other, nt)}

    def part(step):
        return pltpu.make_async_remote_copy(
            fed_ref.at[lax.rem(me + step, group)],
            landing.at[step],
            send.at[step],
            recv.at[step],
            where(step),
            MESH,
        )

    def spread(step, slot):
        return pltpu.make_async_remote_copy(
            out_ref.at[slot],
            out_ref.at[slot],
            send2.at[step],
            recv2.at[step],
            {"sp": sp, "tp": lax.rem(tp + step, nt)},
            MESH,
        )

    greet(group, where)
    for step in range(1, group):
        part(step).start()
    for step in range(1, group):
        part(step).wait_recv()
    chunk = 16

    @pl.loop(0, rows // chunk)
    def _(i):
        at = pl.ds(pl.multiple_of(i * chunk, chunk), chunk)
        fed = fed_ref[me, at].astype(jnp.float32)
        for step in range(1, group):
            fed = fed + landing[step, at].astype(jnp.float32)
        out_ref[tp, at] = (resid_ref[at] + fed).astype(jnp.bfloat16)

    for step in range(1, nt):
        spread(step, tp).start()
    for step in range(1, nt):
        copy = spread(step, lax.rem(tp + nt - step, nt))
        copy.wait_recv()
        copy.wait_send()
    for step in range(1, group):
        part(step).wait_send()


def last_stage(nt, fed, resid):
    rows, width = resid.shape
    return pl.pallas_call(
        functools.partial(last_kernel, nt),
        out_shape=jax.ShapeDtypeStruct((nt, rows, width), jnp.bfloat16),
        in_specs=[VM, VM],
        out_specs=VM,
        scratch_shapes=[pltpu.VMEM((2 * nt, rows, width), jnp.bfloat16)]
        + [pltpu.SemaphoreType.DMA((2 * nt,))] * 2
        + [pltpu.SemaphoreType.DMA((nt,))] * 2,
        compiler_params=params(2),
        name="last_stage",
    )(fed.reshape(2 * nt, rows, width), resid)


def pair_share(n, arrays, axis, joins):
    side = lax.rem(lax.axis_index("sp"), 2)
    own, away = [], []
    for array in arrays:
        half = array.shape[axis] // 2
        own.append(lax.dynamic_slice_in_dim(array, side * half, half, axis))
        away.append(lax.dynamic_slice_in_dim(array, (1 - side) * half, half, axis))
    own = jnp.concatenate(own, axis=axis)
    away = jnp.concatenate(away, axis=axis)
    came = lax.ppermute(away, "sp", [(i, i ^ 1) for i in range(n)])
    first = jnp.where(side == 0, own, came)
    second = jnp.where(side == 0, came, own)
    return jnp.concatenate([first, second], axis=joins)


def per_device(
    n,
    nt,
    tokens_in,
    queries,
    keys,
    values,
    doc_ids,
    query_gain,
    key_norm_scale,
    out_weight,
    norm_gain,
    gate_weight,
    up_weight,
    down_weight,
):
    tok_rows = tokens_in.shape[0]
    head_dim = query_gain.shape[0]
    local_heads = queries.shape[1] // head_dim
    places = lax.axis_index("sp") * tok_rows + jnp.arange(tok_rows, dtype=jnp.int32)
    lattice_row = (places // GRID).astype(jnp.float32)
    lattice_column = (places % GRID).astype(jnp.float32)
    q_local = normalized_rotated(queries, query_gain, local_heads, lattice_row, lattice_column)
    q_rows = q_local.transpose(1, 0, 2).reshape(local_heads * tok_rows, head_dim)
    lanes = [[2 * j + side for j in range(n // 2)] for side in range(2)]
    gate_up_all = lax.all_gather(
        pair_share(n, [gate_weight, up_weight], 1, 0), "sp", axis_index_groups=lanes, axis=0, tiled=True
    )
    down_all = lax.all_gather(
        pair_share(n, [down_weight], 0, 1), "sp", axis_index_groups=lanes, axis=1, tiled=True
    )
    turned = normalized_rotated(keys, key_norm_scale, 1, lattice_row, lattice_column)
    packed = jnp.concatenate([turned.reshape(tok_rows, head_dim), values], axis=1)
    kv_all, doc_all = gather_sp(n, packed, doc_ids.reshape(1, tok_rows))
    row_docs = jnp.tile(doc_ids, local_heads)
    first_doc = doc_ids[0]
    last_doc = doc_ids[-1]
    scale = head_dim ** (-0.5)
    total_rows = local_heads * tok_rows

    def absorb_block(state, key_block, value_block, doc_block):

        def absorb(current):
            running_max, running_sum, running_acc = current
            scores = (
                jnp.einsum("qd,kd->qk", q_rows, key_block, preferred_element_type=jnp.float32)
                * scale
            )
            same = row_docs[:, None] == doc_block[None, :]
            scores = jnp.where(same, scores, NEG)
            new_max = jnp.maximum(running_max, jnp.max(scores, axis=1))
            weights = jnp.where(same, jnp.exp(scores - new_max[:, None]), 0.0)
            shrink = jnp.exp(running_max - new_max)
            new_sum = running_sum * shrink + jnp.sum(weights, axis=1)
            new_acc = running_acc * shrink[:, None] + jnp.dot(
                weights.astype(jnp.bfloat16), value_block, preferred_element_type=jnp.float32
            )
            return (new_max, new_sum, new_acc)

        touches = (doc_block[0] <= last_doc) & (doc_block[-1] >= first_doc)
        return lax.cond(touches, absorb, lambda current: current, state)

    initial = (
        jnp.full((total_rows,), NEG, jnp.float32),
        jnp.zeros((total_rows,), jnp.float32),
        jnp.zeros((total_rows, head_dim), jnp.float32),
    )
    carry = initial
    shards = n
    joined = 1
    while joined * 2 <= shards and shards % (joined * 2) == 0 and (joined * 2 * tok_rows <= 1024):
        joined = joined * 2
    blocks = shards // joined
    span_rows = joined * tok_rows
    key_blocks = kv_all[..., :head_dim].reshape(blocks, span_rows, head_dim)
    value_blocks = kv_all[..., head_dim:].reshape(blocks, span_rows, head_dim)
    doc_blocks = doc_all.reshape(blocks, span_rows)

    def visit(state, inputs):
        key_block, value_block, doc_block = inputs
        return (absorb_block(state, key_block, value_block, doc_block), None)

    carry, unused = lax.scan(visit, carry, (key_blocks, value_blocks, doc_blocks))
    attended = (carry[2] / carry[1][:, None]).astype(jnp.bfloat16)
    attended = (
        attended.reshape(local_heads, tok_rows, head_dim)
        .transpose(1, 0, 2)
        .reshape(tok_rows, local_heads * head_dim)
    )
    partial_value = jnp.dot(attended, out_weight, preferred_element_type=jnp.float32)
    normed, resid = mid_stage(nt, partial_value.astype(jnp.bfloat16), tokens_in, norm_gain)
    normed = normed.reshape(2 * tok_rows, -1)
    both = jnp.dot(normed, gate_up_all, preferred_element_type=jnp.float32)
    units = both.shape[1] // 2
    hidden = (jax.nn.silu(both[:, :units]) * both[:, units:]).astype(jnp.bfloat16)
    fed_part = jnp.dot(hidden, down_all, preferred_element_type=jnp.float32)
    out = last_stage(nt, fed_part.astype(jnp.bfloat16), resid)
    return out.reshape(tok_rows, -1)


def solution(mesh):
    return jax.shard_map(
        functools.partial(per_device, mesh.shape["sp"], mesh.shape["tp"]),
        mesh=mesh,
        in_specs=(
            P("sp", None),
            P("sp", "tp"),
            P("sp", "tp"),
            P("sp", "tp"),
            P("sp"),
            P(),
            P(),
            P("tp", None),
            P(),
            P("sp", "tp"),
            P("sp", "tp"),
            P("tp", "sp"),
        ),
        out_specs=P("sp", None),
        check_vma=False,
    )
```

profile of v0, /device:TPU:0, one launch (start us, length us, event | category | flops | bytes accessed | tf_op | source)
XLA Modules:
  0.0 261.3 jit_solution(7590346824540702344)
XLA Ops:
  6.5 2.2 constant_dynamic-slice_fusion.5
  8.8 0.2 pad_maximum_fusion.2
  9.0 3.1 %collective-permute-start = (bf16[256,1408]{1,0:T(8,128)(2,1)S(1)}, bf16[256,1408]{1,0:T(8,128)(2,1)S(1)}, u32[]{:S(2)}, u32[]{:S(2)}) collective-permute-start(bf16[256,1408]{1,0:T(8,128)(2,1)S(1)} %pad_maximum_fusion.2), channel_id=1, source_target_pairs={{0,4},{4,0},{8,12},{12,8},{16,20},{20,16},{24,28},{28,24},{1,5},{5... | collective-permute-start | bytes 2162696 | tf_op jit(solution)/shard_map/ppermute | solution.py:264
  12.0 16.1 %collective-permute-done = bf16[256,1408]{1,0:T(8,128)(2,1)S(1)} collective-permute-done((bf16[256,1408]{1,0:T(8,128)(2,1)S(1)}, bf16[256,1408]{1,0:T(8,128)(2,1)S(1)}, u32[]{:S(2)}, u32[]{:S(2)}) %collective-permute-start) | collective-permute-done | bytes 720928 | tf_op jit(solution)/shard_map/ppermute | solution.py:264
  28.2 0.4 broadcast_select_fusion.1
  28.6 1.2 pad_maximum_fusion
  29.8 0.0 all-gather.3.cloned.1.call-update
  29.8 0.0 all-gather.5.cloned.1.call-start
  30.0 0.0 copy-start.7
  30.0 1.8 collective-permute-start.1
  31.8 7.8 %collective-permute-done.1 = bf16[704,256]{1,0:T(8,128)(2,1)S(1)} collective-permute-done((bf16[704,256]{1,0:T(8,128)(2,1)S(1)}, bf16[704,256]{1,0:T(8,128)(2,1)S(1)}, u32[]{:S(2)}, u32[]{:S(2)}) %collective-permute-start.1) | collective-permute-done | bytes 360480 | tf_op jit(solution)/shard_map/ppermute | solution.py:264
  39.6 0.2 broadcast_select_fusion.3
  39.8 0.9 pad_maximum_fusion.3
  40.7 0.0 all-gather.5.cloned.1.call-update
  40.8 0.1 copy.29
  41.0 0.2 multiply_cosine_fusion.3
  41.2 0.1 fusion.24
  41.3 0.2 copy.33
  41.5 0.1 copy.25
  41.7 0.1 copy.28
  41.8 0.1 fusion.33
  41.9 0.1 fusion.35
  42.0 1.2 fusion.46
  43.3 0.8 concatenate.37.kv_ref
  44.1 23.7 %gather_sp.1 = (bf16[8,256,128]{2,1,0:T(8,128)(2,1)}, s32[8,1,256]{2,1,0:T(1,128)}) custom-call(bf16[256,128]{1,0:T(8,128)(2,1)} %concatenate.37.kv_ref, s32[1,256]{1,0:T(1,128)S(1)} %bitcast.84), custom_call_target="tpu_custom_call" | custom-call | tf_op jit(solution)/shard_map/gather_sp/pallas_call | solution.py:93
  67.8 0.7 reduce.2
  68.5 0.6 fusion.54
  69.1 1.4 fusion.53
  70.6 13.3 %while.15 = (s32[]{:T(128)}, f32[1024]{0:T(1024)S(1)}, f32[1024]{0:T(1024)S(1)}, f32[1024,64]{0,1:T(8,128)S(1)}, s32[2,1024]{1,0:T(2,128)S(1)}, /*index=5*/s32[]...) while((s32[]{:T(128)}, f32[1024]{0:T(1024)S(1)}, ...), condition=%wide.region_7.8_spmd.clone, body=%wide.region_2.7_spmd.clone.sunk | while | flops 285345792 | bytes 14005583 | solution.py:352
  70.6 0.6 fusion.63
  73.7 3.6 %conditional.3 = ((f32[1024]{0:T(1024)S(1)}, f32[1024]{0:T(1024)S(1)}, f32[1024,64]{0,1:T(8,128)S(1)})) conditional(s32[]{:T(128)} %convert_element_type.71, (f32[1024]{0:T(1024)S(1)}, f32[1024]{0:T(1024)S(1)}, f32[1024,64]{0,1:T(8,128)S(1)}) %tuple.64, (s32[256]{0:T(256)S(1)}, s32[1,1024]{1,0:T(1,128)S(1)}, bf16[2,1024,64]{2,1,0:T(8,128)(2,1)S(1)}, ...), branch_computations={%region_3.3_spmd, %region_4.6_spmd} | conditional | flops 285345792 | bytes 13997096 | solution.py:330
  73.7 0.7 fusion.2
  74.5 1.5 fusion.4
  76.0 1.2 fusion.7
  77.3 0.6 fusion.63
  80.3 3.6 %conditional.3 = ((f32[1024]{0:T(1024)S(1)}, f32[1024]{0:T(1024)S(1)}, f32[1024,64]{0,1:T(8,128)S(1)})) conditional(s32[]{:T(128)} %convert_element_type.71, (f32[1024]{0:T(1024)S(1)}, f32[1024]{0:T(1024)S(1)}, f32[1024,64]{0,1:T(8,128)S(1)}) %tuple.64, (s32[256]{0:T(256)S(1)}, s32[1,1024]{1,0:T(1,128)S(1)}, bf16[2,1024,64]{2,1,0:T(8,128)(2,1)S(1)}, ...), branch_computations={%region_3.3_spmd, %region_4.6_spmd} | conditional | flops 285345792 | bytes 13997096 | solution.py:330
  80.4 0.7 fusion.2
  81.1 1.5 fusion.4
  82.7 1.2 fusion.7
  84.0 0.1 reshape.342
  84.1 1.4 convolution_convert_fusion.1
  85.5 37.4 %mid_stage.1 = (bf16[8,64,2048]{2,1,0:T(8,128)(2,1)}, f32[64,2048]{1,0:T(8,128)}) custom-call(bf16[4,64,2048]{2,1,0:T(8,128)(2,1)} %bitcast.70, bf16[4,64,2048]{2,1,0:T(8,128)(2,1)} %bitcast.72, f32[1,2048]{1,0:T(1,128)} %bitcast.85), custom_call_target="tpu_custom_call" | custom-call | tf_op jit(solution)/shard_map/mid_stage/pallas_call | solution.py:167
  123.0 26.4 %all-gather.3.cloned.1.call-done = bf16[2048,1408]{1,0:T(8,128)(2,1)} async-done(((bf16[512,1408]{1,0:T(8,128)(2,1)}), bf16[2048,1408]{1,0:T(8,128)(2,1)}) %all-gather.3.cloned.1.call-update) | async-done | bytes 5767184 | tf_op jit(solution)/shard_map/all_gather | solution.py:295
  149.4 8.3 %fusion.55 = f32[512,1408]{1,0:T(8,128)} fusion(bf16[512,2048]{1,0:T(8,128)(2,1)} %bitcast.86, bf16[2048,1408]{1,0:T(8,128)(2,1)} %all-gather.3.cloned.1.call-done), kind=kOutput, calls=%fused_computation.101 | convolution fusion | flops 2952790016 | bytes 10747904 | tf_op jit(solution)/shard_map/dot_general | solution.py:362
  157.7 50.7 %all-gather.5.cloned.1.call-done = bf16[704,2048]{1,0:T(8,128)(2,1)} async-done(((bf16[704,512]{1,0:T(8,128)(2,1)}), bf16[704,2048]{1,0:T(8,128)(2,1)}) %all-gather.5.cloned.1.call-update) | async-done | bytes 2883600 | tf_op jit(solution)/shard_map/all_gather | solution.py:298
  208.3 6.0 %convolution_convert_fusion = bf16[512,2048]{1,0:T(8,128)(2,1)} fusion(bf16[704,2048]{1,0:T(8,128)(2,1)} %all-gather.5.cloned.1.call-done, f32[512,1408]{1,0:T(8,128)} %fusion.55), kind=kOutput, calls=%fused_computation.23 | convolution fusion | flops 1479606272 | bytes 8126464 | tf_op jit(solution)/shard_map/dot_general | solution.py:365
  214.3 37.9 %last_stage.1 = bf16[4,64,2048]{2,1,0:T(8,128)(2,1)} custom-call(bf16[8,64,2048]{2,1,0:T(8,128)(2,1)} %bitcast.71, f32[64,2048]{1,0:T(8,128)} %get-tuple-element.156.resid_ref), custom_call_target="tpu_custom_call" | custom-call | tf_op jit(solution)/shard_map/last_stage/pallas_call | solution.py:242
  252.2 2.3 copy.55
  (42 shorter events, 0.3 us)
Async XLA Ops:
  6.5 77.5 %copy-start = (bf16[256,2048]{1,0:T(8,128)(2,1)S(1)}, bf16[256,2048]{1,0:T(8,128)(2,1)}, u32[]{:S(2)}) copy-start(bf16[256,2048]{1,0:T(8,128)(2,1)} %param.23) | copy-start | bytes 3145732
  6.5 142.8 %all-gather.3.cloned.1.call-start = ((), (), s32[]{:S(2)}) async-start(), calls=%async_computation | async-start | bytes 7208960 | tf_op jit(solution)/shard_map/all_gather | solution.py:295
  9.0 19.2 %collective-permute-start = (bf16[256,1408]{1,0:T(8,128)(2,1)S(1)}, bf16[256,1408]{1,0:T(8,128)(2,1)S(1)}, u32[]{:S(2)}, u32[]{:S(2)}) collective-permute-start(bf16[256,1408]{1,0:T(8,128)(2,1)S(1)} %pad_maximum_fusion.2), channel_id=1, source_target_pairs={{0,4},{4,0},{8,12},{12,8},{16,20},{20,16},{24,28},{28,24},{1,5},{5... | collective-permute-start | bytes 2162696 | tf_op jit(solution)/shard_map/ppermute | solution.py:264
  28.6 1.3 copy-start.1
  29.8 11.0 %copy-start.2 = (bf16[256,256]{1,0:T(8,128)(2,1)S(1)}, bf16[256,256]{1,0:T(8,128)(2,1)}, u32[]{:S(2)}) copy-start(bf16[256,256]{1,0:T(8,128)(2,1)} %param.17) | copy-start | bytes 393220
  29.8 11.4 %copy-start.6 = (f32[64]{0:T(128)S(1)}, f32[64]{0:T(128)}, u32[]{:S(2)}) copy-start(f32[64]{0:T(128)} %param.21) | copy-start | bytes 772
  29.8 178.5 %all-gather.5.cloned.1.call-start = ((), (), s32[]{:S(2)}) async-start(), calls=%async_computation.1 | async-start | bytes 3604480 | tf_op jit(solution)/shard_map/all_gather | solution.py:298
  29.9 11.6 %copy-start.4 = (bf16[256,64]{0,1:T(8,128)(2,1)S(1)}, bf16[256,64]{0,1:T(8,128)(2,1)}, u32[]{:S(2)}) copy-start(bf16[256,64]{0,1:T(8,128)(2,1)} %param.18) | copy-start | bytes 98308
  30.0 11.7 %copy-start.5 = (bf16[256,64]{0,1:T(8,128)(2,1)S(1)}, bf16[256,64]{0,1:T(8,128)(2,1)}, u32[]{:S(2)}) copy-start(bf16[256,64]{0,1:T(8,128)(2,1)} %param.19) | copy-start | bytes 98308
  30.0 12.0 %copy-start.7 = (f32[64]{0:T(128)S(1)}, f32[64]{0:T(128)}, u32[]{:S(2)}) copy-start(f32[64]{0:T(128)} %param.22) | copy-start | bytes 772
  30.0 9.6 %collective-permute-start.1 = (bf16[704,256]{1,0:T(8,128)(2,1)S(1)}, bf16[704,256]{1,0:T(8,128)(2,1)S(1)}, u32[]{:S(2)}, u32[]{:S(2)}) collective-permute-start(bf16[704,256]{1,0:T(8,128)(2,1)S(1)} %constant_dynamic-slice_fusion.2), channel_id=1, source_target_pairs={{0,4},{4,0},{8,12},{12,8},{16,20},{20,16},{24,28},{28,24},{1,5},{5... | collective-permute-start | bytes 1081352 | tf_op jit(solution)/shard_map/ppermute | solution.py:264
  39.8 4.2 %copy-start.3 = (s32[256]{0:T(256)S(1)}, s32[256]{0:T(256)}, u32[]{:S(2)}) copy-start(s32[256]{0:T(256)} %param.20) | copy-start | bytes 3076
Sparse Core Ops, SparseCore 0:
  30.0 119.3 all-gather.2
  151.0 57.3 all-gather.4
where the time goes:
time: 264 us; the launch traced here: 261 us
  waiting for transfers between devices  101 us (38%)
  Pallas kernels  99 us (38%)
  matrix products  19.6 us (7%)
  between operations  13.7 us (5%)
  local copies, waits for them, and re-layouts  9.25 us (4%)
  other arithmetic  8.65 us (3%)
  loops' own time  5.11 us (2%)
  starting transfers between devices  4.91 us (2%)
    all_gather x1, waiting for transfers between devices, per_device(): lax.all_gather(pair_share(n, [down_weight], 0, 1), 'sp', axis_index_group...  50.7 us
    pallas_call x1, Pallas kernels, last_stage(): pl.pallas_call(functools.partial(last_kernel, nt), out_shape=jax.ShapeDty...  37.9 us
    pallas_call x1, Pallas kernels, mid_stage(): pl.pallas_call(functools.partial(mid_kernel, nt), out_shape=(jax.ShapeDty...  37.4 us
    all_gather x1, waiting for transfers between devices, per_device(): lax.all_gather(pair_share(n, [gate_weight, up_weight], 1, 0), 'sp', axis_...  26.4 us
    ppermute x2, waiting for transfers between devices, pair_share(): came = lax.ppermute(away, 'sp', [(i, i ^ 1) for i in range(n)])  24 us
    pallas_call x1, Pallas kernels, gather_sp(): pl.pallas_call(functools.partial(gather_kernel, n), out_shape=(jax.ShapeD...  23.7 us
    dot_general x1, matrix products, per_device(): both = jnp.dot(normed, gate_up_all, preferred_element_type=jnp.float32)  8.29 us
    dot_general x1, matrix products, per_device(): fed_part = jnp.dot(hidden, down_all, preferred_element_type=jnp.float32)  5.97 us
  transfers between devices with their start and end apart: 4, of which 4 were waited for; matrix products, arithmetic and copies ran while one was open for 10% of the time, Pallas kernels for 23%

commit v1 on v0

--- a/solution.py
+++ b/solution.py
@@ -265,6 +265,676 @@
     first = jnp.where(side == 0, own, came)
     second = jnp.where(side == 0, came, own)
     return jnp.concatenate([first, second], axis=joins)
+
+
+SIDES = 2
+LANE = 128
+
+
+def turned(block, gain, table):
+    power = jnp.mean(block * block, axis=0, keepdims=True)
+    full = block * lax.rsqrt(power + EPS) * gain
+    half = block.shape[0] // 2
+    quarter = half // 2
+    pieces = []
+    for part in range(2):
+        first = full[part * half : part * half + quarter]
+        second = full[part * half + quarter : (part + 1) * half]
+        cosine = table[2 * part * quarter : (2 * part + 1) * quarter]
+        sine = table[(2 * part + 1) * quarter : (2 * part + 2) * quarter]
+        pieces += [first * cosine - second * sine, second * cosine + first * sine]
+    return jnp.concatenate(pieces, axis=0)
+
+
+def fused_kernel(
+    n,
+    nt,
+    wide,
+    q_in,
+    k_in,
+    v_in,
+    doc_in,
+    table_in,
+    q_gain,
+    k_gain,
+    norm_gain,
+    tokens,
+    out_weight,
+    gate,
+    up,
+    down,
+    out,
+    kv,
+    q_ref,
+    top,
+    total,
+    acc,
+    att_out,
+    att,
+    ow,
+    tok,
+    resid,
+    act,
+    gw,
+    uw,
+    dw,
+    hid,
+    keep,
+    core_out,
+    core_in,
+    x_keep,
+    x_out,
+    x_in,
+    z_keep,
+    z_out,
+    z_in,
+    kv_zs,
+    kv_ys,
+    kv_r,
+    w_own,
+    w_zs,
+    w_ys,
+    w_r,
+    misc,
+    ow_xs,
+    ow_cs,
+    ow_r,
+    att_s,
+    att_r,
+    act_us,
+    act_ds,
+    act_xs,
+    act_cs,
+    act_r,
+    rs_cs,
+    rs_cr,
+    rs_xs,
+    rs_xr,
+    rs_zs,
+    rs_zr,
+    ag_xs,
+    ag_cs,
+    ag_r,
+):
+    sp, tp = lax.axis_index("sp"), lax.axis_index("tp")
+    lanes, xs = n // SIDES, nt // 2
+    lane, side = sp // SIDES, sp % SIDES
+    xi, core = tp // 2, tp % 2
+    rows = q_in.shape[1]
+    head_dim = k_in.shape[0]
+    heads = q_in.shape[0] // head_dim
+    chunk = rows // nt
+    blocks = gate.shape[1] // LANE
+    width = wide * LANE
+    cut = lanes * wide - blocks
+    kv_docs = head_dim
+    kv_vals = kv.shape[1] - head_dim
+
+    def at_sp(lane_to, side_to):
+        return {"sp": lane_to * SIDES + side_to, "tp": tp}
+
+    def at_tp(x_to, core_to):
+        return {"sp": sp, "tp": x_to * 2 + core_to}
+
+    def remote(src, dst, send, recv, where):
+        return pltpu.make_async_remote_copy(src, dst, send, recv, where, MESH)
+
+    def lane_at(d):
+        return (lane + d) % lanes
+
+    def x_at(d):
+        return (xi + d) % xs
+
+    other_side = 1 - side
+    other_core = 1 - core
+
+    barrier = pltpu.get_barrier_semaphore()
+    for d in range(1, lanes):
+        pl.semaphore_signal(barrier, inc=1, device_id=at_sp(lane_at(d), side), device_id_type=MESH)
+    pl.semaphore_signal(barrier, inc=1, device_id=at_sp(lane, other_side), device_id_type=MESH)
+    for d in range(1, nt):
+        pl.semaphore_signal(
+            barrier, inc=1, device_id={"sp": sp, "tp": (tp + d) % nt}, device_id_type=MESH
+        )
+
+    def unit_from(lane_to):
+        return pl.multiple_of((lane_to * wide - (lane_to // (lanes - 1)) * cut) * LANE, LANE)
+
+    def weight_block(m, lane_to):
+        at = pl.ds(unit_from(lane_to), width)
+        if m == 0:
+            return gate.at[:, at]
+        if m == 1:
+            return up.at[:, at]
+        return down.at[at, :]
+
+    landed = (gw, uw, dw)
+
+    own_copies = [
+        pltpu.make_async_copy(weight_block(m, lane), landed[m].at[sp], w_own.at[m]) for m in range(3)
+    ]
+    own_copies.append(pltpu.make_async_copy(out_weight, ow.at[tp], misc.at[0]))
+    own_copies.append(
+        pltpu.make_async_copy(tokens.at[pl.ds(pl.multiple_of(tp * chunk, chunk), chunk)], tok, misc.at[1])
+    )
+    for copy in own_copies:
+        copy.start()
+
+    kv[sp, 0:head_dim, :] = turned(k_in[...].astype(jnp.float32), k_gain[...], table_in[...]).astype(
+        jnp.bfloat16
+    )
+    kv[sp, kv_docs:kv_vals, :] = doc_in[...]
+    kv[sp, kv_vals:, :] = v_in[...]
+
+    pl.semaphore_wait(barrier, lanes - 1 + 1 + nt - 1)
+
+    def kv_z(d, slot):
+        return remote(kv.at[slot], kv.at[slot], kv_zs.at[d], kv_r.at[slot], at_sp(lane_at(d), side))
+
+    def kv_y(lane_of, side_of):
+        slot = lane_of * SIDES + side_of
+        return remote(
+            kv.at[slot], kv.at[slot], kv_ys.at[lane_of], kv_r.at[slot], at_sp(lane, other_side)
+        )
+
+    for d in range(1, lanes):
+        kv_z(d, sp).start()
+    kv_y(lane, side).start()
+
+    def ow_x(d):
+        return remote(out_weight, ow.at[tp], ow_xs.at[d], ow_r.at[tp], at_tp(x_at(d), core))
+
+    def ow_core(x_of, core_of):
+        slot = x_of * 2 + core_of
+        return remote(ow.at[slot], ow.at[slot], ow_cs.at[x_of], ow_r.at[slot], at_tp(xi, other_core))
+
+    for d in range(1, xs):
+        ow_x(d).start()
+    own_copies[3].wait()
+    ow_core(xi, core).start()
+
+    scale = head_dim ** (-0.5)
+    for h in range(heads):
+        at = slice(h * head_dim, (h + 1) * head_dim)
+        query = turned(q_in[at, :].astype(jnp.float32), q_gain[...], table_in[...])
+        q_ref[at, :] = (query.astype(jnp.bfloat16).astype(jnp.float32) * scale).astype(jnp.bfloat16)
+    top[...] = jnp.full(top.shape, NEG, jnp.float32)
+    total[...] = jnp.zeros(total.shape, jnp.float32)
+    acc[...] = jnp.zeros(acc.shape, jnp.float32)
+
+    for d in range(1, lanes):
+        slot = lane_at(-d) * SIDES + side
+        kv_z(d, slot).wait_recv()
+        kv_y(lane_at(-d), side).start()
+
+    def w_z(m, d, slot):
+        return remote(
+            weight_block(m, lane_at(d)),
+            landed[m].at[slot],
+            w_zs.at[m, d],
+            w_r.at[m, slot],
+            at_sp(lane_at(d), side),
+        )
+
+    def w_y(m, lane_of, side_of):
+        slot = lane_of * SIDES + side_of
+        return remote(
+            landed[m].at[slot],
+            landed[m].at[slot],
+            w_ys.at[m, lane_of],
+            w_r.at[m, slot],
+            at_sp(lane, other_side),
+        )
+
+    for m in range(3):
+        for d in range(1, lanes):
+            w_z(m, d, sp).start()
+        own_copies[m].wait()
+        w_y(m, lane, side).start()
+
+    eye = (
+        lax.broadcasted_iota(jnp.int32, (rows, rows), 0)
+        == lax.broadcasted_iota(jnp.int32, (rows, rows), 1)
+    ).astype(jnp.bfloat16)
+    across = (((1,), (1,)), ((), ()))
+    q_doc = doc_in[0:1, :].astype(jnp.float32)
+
+    @pl.loop(0, n)
+    def _(k):
+        lane_of = (lane + k) % lanes
+        side_of = (side + k // lanes) % SIDES
+        slot = lane_of * SIDES + side_of
+
+        @pl.when(k >= lanes)
+        def _():
+            kv_y(lane_of, side_of).wait_recv()
+
+        upright = lax.dot_general(eye, kv[slot, 0:kv_vals, :], across, preferred_element_type=jnp.float32)
+        key = upright[:, 0:head_dim].astype(jnp.bfloat16)
+        same = upright[:, head_dim : head_dim + 1] == q_doc
+        value = kv[slot, kv_vals:, :]
+        for h in range(heads):
+            at = slice(h * head_dim, (h + 1) * head_dim)
+            scores = jnp.dot(key, q_ref[at, :], preferred_element_type=jnp.float32)
+            scores = jnp.where(same, scores, NEG)
+            before = top[h]
+            now = jnp.maximum(before, jnp.max(scores, axis=0, keepdims=True))
+            weights = jnp.exp(scores - now)
+            shrink = jnp.exp(before - now)
+            top[h] = now
+            total[h] = total[h] * shrink + jnp.sum(weights, axis=0, keepdims=True)
+            acc[at, :] = acc[at, :] * shrink + jnp.dot(
+                value, weights.astype(jnp.bfloat16), preferred_element_type=jnp.float32
+            )
+
+    pieces = []
+    for h in range(heads):
+        at = slice(h * head_dim, (h + 1) * head_dim)
+        pieces.append((acc[at, :] / total[h]).astype(jnp.bfloat16))
+    standing = jnp.concatenate(pieces, axis=0)
+    attended = lax.dot_general(eye, standing, across, preferred_element_type=jnp.float32).astype(
+        jnp.bfloat16
+    )
+    for i in range(nt):
+        att_out[i] = attended[i * chunk : (i + 1) * chunk]
+
+    def att_copy(d, peer, slot):
+        return remote(
+            att_out.at[peer], att.at[slot], att_s.at[d], att_r.at[slot], {"sp": sp, "tp": peer}
+        )
+
+    for d in range(1, nt):
+        att_copy(d, (tp + d) % nt, tp).start()
+    att[tp] = att_out[tp]
+
+    def project(slot):
+        return (
+            jnp.dot(att[slot], ow[slot], preferred_element_type=jnp.float32)
+            .astype(jnp.bfloat16)
+            .astype(jnp.float32)
+        )
+
+    own_copies[4].wait()
+    resid[...] = tok[...].astype(jnp.float32) + project(tp)
+    for d in range(1, nt):
+        slot = (tp + nt - d) % nt
+        att_copy(d, tp, slot).wait_recv()
+    ow_core(xi, other_core).wait_recv()
+    resid[...] += project(xi * 2 + other_core)
+    for d in range(1, xs):
+        x_of = x_at(xs - d)
+        remote(out_weight, ow.at[x_of * 2 + core], ow_xs.at[d], ow_r.at[x_of * 2 + core], at_tp(x_of, core)).wait_recv()
+        ow_core(x_of, core).start()
+        resid[...] += project(x_of * 2 + core)
+    for d in range(1, xs):
+        x_of = x_at(xs - d)
+        ow_core(x_of, other_core).wait_recv()
+        resid[...] += project(x_of * 2 + other_core)
+
+    whole = resid[...]
+    power = jnp.mean(whole * whole, axis=-1, keepdims=True)
+    act[lane, tp] = (whole * lax.rsqrt(power + EPS) * norm_gain[...]).astype(jnp.bfloat16)
+
+    def act_up(lane_of):
+        return remote(
+            act.at[lane_of, tp],
+            act.at[lane_of, tp],
+            act_us.at[lane_of],
+            act_r.at[lane_of, tp],
+            at_sp(lane + 1, side),
+        )
+
+    def act_down(lane_of):
+        return remote(
+            act.at[lane_of, tp],
+            act.at[lane_of, tp],
+            act_ds.at[lane_of],
+            act_r.at[lane_of, tp],
+            at_sp(lane - 1, side),
+        )
+
+    def act_x(d, lane_of, slot):
+        return remote(
+            act.at[lane_of, slot],
+            act.at[lane_of, slot],
+            act_xs.at[d, lane_of],
+            act_r.at[lane_of, slot],
+            at_tp(x_at(d), core),
+        )
+
+    def act_core(lane_of, x_of, core_of):
+        slot = x_of * 2 + core_of
+        return remote(
+            act.at[lane_of, slot],
+            act.at[lane_of, slot],
+            act_cs.at[lane_of, x_of],
+            act_r.at[lane_of, slot],
+            at_tp(xi, other_core),
+        )
+
+    def act_out(lane_of):
+        for d in range(1, xs):
+            act_x(d, lane_of, tp).start()
+        act_core(lane_of, xi, core).start()
+
+    def act_from_x(lane_of):
+        for d in range(1, xs):
+            x_of = x_at(xs - d)
+            act_x(d, lane_of, x_of * 2 + core).wait_recv()
+            act_core(lane_of, x_of, core).start()
+
+    rises, falls = lane < lanes - 1, lane > 0
+
+    @pl.when(rises)
+    def _():
+        act_up(lane).start()
+
+    @pl.when(falls)
+    def _():
+        act_down(lane).start()
+
+    act_out(lane)
+
+    def forward_weight(m):
+        for d in range(1, lanes):
+            lane_of = lane_at(lanes - d)
+            w_z(m, d, lane_of * SIDES + side).wait_recv()
+            w_y(m, lane_of, side).start()
+
+    forward_weight(0)
+    for d in range(1, lanes):
+
+        @pl.when(lane >= d)
+        def _():
+            act_up(lane - d).wait_recv()
+
+            @pl.when(rises)
+            def _():
+                act_up(lane - d).start()
+
+            act_out(lane - d)
+
+        @pl.when(lane + d < lanes)
+        def _():
+            act_down(lane + d).wait_recv()
+
+            @pl.when(falls)
+            def _():
+                act_down(lane + d).start()
+
+            act_out(lane + d)
+
+        if d == 1:
+            act_from_x(lane)
+    forward_weight(1)
+    for d in range(1, lanes):
+
+        @pl.when(lane >= d)
+        def _():
+            act_from_x(lane - d)
+
+        @pl.when(lane + d < lanes)
+        def _():
+            act_from_x(lane + d)
+
+    for m in range(2):
+        for d in range(lanes):
+            w_y(m, lane_at(d), other_side).wait_recv()
+
+    unit = lax.broadcasted_iota(jnp.int32, (nt * chunk, width), 1)
+    mine = unit >= (lane // (lanes - 1)) * cut * LANE
+    for d in range(lanes):
+        lane_of = lane_at(d)
+        for x_of in range(xs):
+            act_core(lane_of, x_of, other_core).wait_recv()
+
+    @pl.loop(0, lanes)
+    def _(lane_of):
+        inputs = act[lane_of].reshape(nt * chunk, act.shape[-1])
+        gated = jnp.dot(inputs, gw[...].reshape(n * gw.shape[1], width), preferred_element_type=jnp.float32)
+        lifted = jnp.dot(inputs, uw[...].reshape(n * uw.shape[1], width), preferred_element_type=jnp.float32)
+        hidden = gated * lax.logistic(gated) * lifted
+        hidden = jnp.where(mine, hidden, 0.0).astype(jnp.bfloat16)
+        for x_of in range(xs):
+            for core_of in range(2):
+                start = (x_of * 2 + core_of) * chunk
+                hid[core_of, x_of, lane_of] = hidden[start : start + chunk]
+
+    cols = dw.shape[2]
+    share = xs * lanes * chunk
+
+    def rs_core(s):
+        return remote(core_out.at[s], core_in.at[s], rs_cs.at[s], rs_cr.at[s], at_tp(xi, other_core))
+
+    def rs_x(s, d):
+        return remote(x_out.at[s, d], x_in.at[s, d], rs_xs.at[s, d], rs_xr.at[s, d], at_tp(x_at(d), core))
+
+    def rs_z(s, d):
+        return remote(
+            z_out.at[s, d], z_in.at[s, d], rs_zs.at[s, d], rs_zr.at[s, d], at_sp(lane_at(d), side)
+        )
+
+    def columns(s):
+        return pl.ds(pl.multiple_of(s * cols, cols), cols)
+
+    def ag_x(s, d, slot):
+        piece = out.at[slot, :, columns(s)]
+        return remote(piece, piece, ag_xs.at[s, d], ag_r.at[s, slot], at_tp(x_at(d), core))
+
+    def ag_core(s, x_of, core_of):
+        slot = x_of * 2 + core_of
+        piece = out.at[slot, :, columns(s)]
+        return remote(piece, piece, ag_cs.at[s, x_of], ag_r.at[s, slot], at_tp(xi, other_core))
+
+    def slot_of(k):
+        return (k // SIDES) * SIDES + (side + k) % SIDES
+
+    @pl.loop(0, n + 4)
+    def _(k):
+        @pl.when(k < n)
+        def _():
+            s = slot_of(k)
+            lane_of, side_of = s // SIDES, s % SIDES
+
+            @pl.when(side_of == side)
+            def _():
+                @pl.when(lane_of != lane)
+                def _():
+                    w_z(2, 1, s).wait_recv()
+                    w_y(2, lane_of, side).start()
+
+            @pl.when(side_of != side)
+            def _():
+                w_y(2, lane_of, other_side).wait_recv()
+
+            away = hid[other_core].reshape(share, width)
+            core_out[s] = (
+                jnp.dot(away, dw[s], preferred_element_type=jnp.float32)
+                .astype(jnp.bfloat16)
+                .reshape(xs, lanes, chunk, cols)
+            )
+            rs_core(s).start()
+            near = hid[core].reshape(share, width)
+            keep[s] = jnp.dot(near, dw[s], preferred_element_type=jnp.float32).reshape(
+                xs, lanes, chunk, cols
+            )
+
+        @pl.when((k >= 1) & (k < n + 1))
+        def _():
+            s = slot_of(k - 1)
+            rs_core(s).wait_recv()
+            for d in range(1, xs):
+                x_to = x_at(d)
+                x_out[s, d] = (keep[s, x_to] + core_in[s, x_to].astype(jnp.float32)).astype(jnp.bfloat16)
+                rs_x(s, d).start()
+            x_keep[s] = keep[s, xi] + core_in[s, xi].astype(jnp.float32)
+
+        @pl.when((k >= 2) & (k < n + 2))
+        def _():
+            s = slot_of(k - 2)
+            for d in range(1, xs):
+                rs_x(s, d).wait_recv()
+
+            def summed(lane_to):
+                value = x_keep[s, lane_to]
+                for d in range(1, xs):
+                    value = value + x_in[s, d, lane_to].astype(jnp.float32)
+                return value
+
+            for d in range(1, lanes):
+                z_out[s, d] = summed(lane_at(d)).astype(jnp.bfloat16)
+                rs_z(s, d).start()
+            z_keep[s] = summed(lane)
+
+        @pl.when((k >= 3) & (k < n + 3))
+        def _():
+            s = slot_of(k - 3)
+            value = z_keep[s]
+            for d in range(1, lanes):
+                rs_z(s, d).wait_recv()
+                value = value + z_in[s, d].astype(jnp.float32)
+            out[tp, :, columns(s)] = (resid[:, columns(s)] + value).astype(jnp.bfloat16)
+            for d in range(1, xs):
+                ag_x(s, d, tp).start()
+            ag_core(s, xi, core).start()
+
+        @pl.when(k >= 4)
+        def _():
+            s = slot_of(k - 4)
+            for d in range(1, xs):
+                x_of = x_at(xs - d)
+                ag_x(s, d, x_of * 2 + core).wait_recv()
+                ag_core(s, x_of, core).start()
+
+    @pl.loop(0, n)
+    def _(s):
+        for x_of in range(xs):
+            ag_core(s, x_of, other_core).wait_recv()
+            ag_core(s, x_of, core).wait_send()
+        for d in range(1, xs):
+            ag_x(s, d, tp).wait_send()
+            rs_x(s, d).wait_send()
+        rs_core(s).wait_send()
+        for d in range(1, lanes):
+            rs_z(s, d).wait_send()
+
+    for d in range(1, lanes):
+        kv_z(d, sp).wait_send()
+        for m in range(3):
+            w_z(m, d, sp).wait_send()
+    for lane_of in range(lanes):
+        kv_y(lane_of, side).wait_send()
+        for m in range(3):
+            w_y(m, lane_of, side).wait_send()
+        for d in range(1, xs):
+            act_x(d, lane_of, tp).wait_send()
+        for x_of in range(xs):
+            act_core(lane_of, x_of, core).wait_send()
+
+        @pl.when(rises & (lane_of <= lane))
+        def _():
+            act_up(lane_of).wait_send()
+
+        @pl.when(falls & (lane_of >= lane))
+        def _():
+            act_down(lane_of).wait_send()
+
+    for d in range(1, xs):
+        ow_x(d).wait_send()
+    for x_of in range(xs):
+        ow_core(x_of, core).wait_send()
+    for d in range(1, nt):
+        att_copy(d, (tp + d) % nt, tp).wait_send()
+
+
+VMEM_LIMIT = 60 * 1024 * 1024
+
+
+def fused_plan(n, nt, rows, width, head_dim, heads, units):
+    if n % SIDES or n < 2 * SIDES or nt % 2 or rows % nt or units % LANE:
+        return None
+    lanes, xs, chunk, blocks = n // SIDES, nt // 2, rows // nt, units // LANE
+    wide = -(-blocks // lanes)
+    cols = width // n
+    if chunk % 16 or rows % LANE or cols % LANE or width % n or head_dim % 32:
+        return None
+    if wide > blocks or (lanes - 1) * wide > blocks:
+        return None
+    wu = wide * LANE
+    bf, f32 = jnp.bfloat16, jnp.float32
+    shapes = [
+        ((n, 2 * head_dim + 16, rows), bf),
+        ((heads * head_dim, rows), bf),
+        ((heads, 1, rows), f32),
+        ((heads, 1, rows), f32),
+        ((heads * head_dim, rows), f32),
+        ((nt, chunk, heads * head_dim), bf),
+        ((nt, chunk, heads * head_dim), bf),
+        ((nt, heads * head_dim, width), bf),
+        ((chunk, width), bf),
+        ((chunk, width), f32),
+        ((lanes, nt, chunk, width), bf),
+        ((n, width // n, wu), bf),
+        ((n, width // n, wu), bf),
+        ((n, wu, cols), bf),
+        ((2, xs, lanes, chunk, wu), bf),
+        ((n, xs, lanes, chunk, cols), f32),
+        ((n, xs, lanes, chunk, cols), bf),
+        ((n, xs, lanes, chunk, cols), bf),
+        ((n, lanes, chunk, cols), f32),
+        ((n, xs, lanes, chunk, cols), bf),
+        ((n, xs, lanes, chunk, cols), bf),
+        ((n, chunk, cols), f32),
+        ((n, lanes, chunk, cols), bf),
+        ((n, lanes, chunk, cols), bf),
+    ]
+    size = 0
+    for shape, kind in shapes:
+        count = 1
+        for extent in shape:
+            count *= extent
+        size += count * jnp.dtype(kind).itemsize
+    if size > VMEM_LIMIT * 3 // 4:
+        return None
+    sems = [(lanes,), (lanes,), (n,), (3,), (3, lanes), (3, lanes), (3, n), (2,)]
+    sems += [(xs,), (xs,), (nt,), (nt,), (nt,)]
+    sems += [(lanes,), (lanes,), (xs, lanes), (lanes, xs), (lanes, nt)]
+    sems += [(n,), (n,), (n, xs), (n, xs), (n, lanes), (n, lanes), (n, xs), (n, xs), (n, nt)]
+    return wide, [pltpu.VMEM(*s) for s in shapes] + [pltpu.SemaphoreType.DMA(s) for s in sems]
+
+
+def fused_layer(
+    n, nt, plan, tokens_in, queries, keys, values, doc_ids, query_gain, key_norm_scale,
+    out_weight, norm_gain, gate_weight, up_weight, down_weight,
+):
+    wide, scratch = plan
+    rows, width = tokens_in.shape
+    head_dim = query_gain.shape[0]
+    places = lax.axis_index("sp") * rows + jnp.arange(rows, dtype=jnp.int32)
+    half = head_dim // 2
+    freqs = THETA ** (-2.0 * jnp.arange(half // 2, dtype=jnp.float32) / half)
+    angles = [
+        freqs[:, None] * spot.astype(jnp.float32)[None, :] for spot in (places // GRID, places % GRID)
+    ]
+    table = jnp.concatenate([f(a) for a in angles for f in (jnp.cos, jnp.sin)], axis=0)
+    docs = jnp.broadcast_to(doc_ids.astype(jnp.bfloat16)[None, :], (16, rows))
+    hbm = pl.BlockSpec(memory_space=pl.ANY)
+    out = pl.pallas_call(
+        functools.partial(fused_kernel, n, nt, wide),
+        out_shape=jax.ShapeDtypeStruct((nt, rows // nt, width), jnp.bfloat16),
+        in_specs=[VM] * 8 + [hbm] * 5,
+        out_specs=VM,
+        scratch_shapes=scratch,
+        compiler_params=pltpu.CompilerParams(
+            collective_id=3, has_side_effects=True, vmem_limit_bytes=VMEM_LIMIT
+        ),
+        name="fused_layer",
+    )(
+        queries.T, keys.T, values.T, docs, table,
+        query_gain.reshape(head_dim, 1), key_norm_scale.reshape(head_dim, 1), norm_gain.reshape(1, width),
+        tokens_in, out_weight, gate_weight, up_weight, down_weight,
+    )
+    return out.reshape(rows, width)
 
 
 def per_device(
@@ -286,6 +956,16 @@
     tok_rows = tokens_in.shape[0]
     head_dim = query_gain.shape[0]
     local_heads = queries.shape[1] // head_dim
+    plan = None
+    if keys.shape[1] == head_dim:
+        plan = fused_plan(
+            n, nt, tok_rows, tokens_in.shape[1], head_dim, local_heads, gate_weight.shape[1]
+        )
+    if plan is not None:
+        return fused_layer(
+            n, nt, plan, tokens_in, queries, keys, values, doc_ids, query_gain, key_norm_scale,
+            out_weight, norm_gain, gate_weight, up_weight, down_weight,
+        )
     places = lax.axis_index("sp") * tok_rows + jnp.arange(tok_rows, dtype=jnp.int32)
     lattice_row = (places // GRID).astype(jnp.float32)
     lattice_column = (places % GRID).astype(jnp.float32)

time: 264 us -> 156 us (0.59); the launches traced: 261 us -> 156 us
  waiting for transfers between devices: 101 us -> 0 us
  Pallas kernels: 99 us -> 150 us
  matrix products: 19.6 us -> 0 us
  between operations: 13.7 us -> 0.04 us
  other arithmetic: 8.65 us -> 0.85 us
  loops' own time: 5.11 us -> 0 us
  starting transfers between devices: 4.91 us -> 0 us
  local copies, waits for them, and re-layouts: 9.25 us -> 5.79 us
    all_gather x2 -> x0, waiting for transfers between devices: 77.1 us -> none  [the longest x1 50.7 us: per_device(): lax.all_gather(pair_share(n, [down_weight], 0, 1), 'sp', axis_index_group...]
    pallas_call x3 -> x1, Pallas kernels: 99 us -> 150 us  [fused_layer(): pl.pallas_call(functools.partial(fused_kernel, n, nt, wide), out_shape=ja...]
    ppermute x2 -> x0, waiting for transfers between devices: 24 us -> none  [pair_share(): came = lax.ppermute(away, 'sp', [(i, i ^ 1) for i in range(n)])]
    dot_general x7 -> x0, matrix products: 19.6 us -> none  [the longest x1 8.29 us: per_device(): both = jnp.dot(normed, gate_up_all, preferred_element_type=jnp.float32)]
    another operation x3 -> x0, loops' own time: 5.11 us -> none  [the longest x1 4.96 us: per_device(): lax.scan(visit, carry, (key_blocks, value_blocks, doc_blocks))]
    ppermute x2 -> x0, starting transfers between devices: 4.86 us -> none  [pair_share(): came = lax.ppermute(away, 'sp', [(i, i ^ 1) for i in range(n)])]
    reduce_sum x4 -> x0, other arithmetic: 3.25 us -> none  [the longest x2 3.09 us: absorb(): new_sum = running_sum * shrink + jnp.sum(weights, axis=1)]
    slice x4 -> x0, local copies, waits for them, and re-layouts: 3.19 us -> none  [the longest x1 1.43 us: per_device(): value_blocks = kv_all[..., head_dim:].reshape(blocks, span_rows, head_dim)]
  transfers between devices with their start and end apart: 4 -> 0, of which waited for: 4 -> 0; matrix products, arithmetic and copies ran while one was open for 10% -> 0% of each run, Pallas kernels for 23% -> 0%
where the time goes in v1:
time: 156 us
  Pallas kernels  150 us (96%)
  local copies, waits for them, and re-layouts  5.79 us (4%)
    pallas_call x1, Pallas kernels, fused_layer(): pl.pallas_call(functools.partial(fused_kernel, n, nt, wide), out_shape=ja...  150 us
    unnamed x10, local copies, waits for them, and re-layouts  3.79 us

profile of v1, /device:TPU:0, one launch (start us, length us, event | category | flops | bytes accessed | tf_op | source)
XLA Modules:
  0.0 156.3 jit_solution(9989609439664850231)
XLA Ops:
  0.0 0.0 copy-start.3
  0.0 0.7 copy-done.3
  0.7 0.0 copy-start.1
  0.7 0.0 copy-start.2
  0.7 0.6 broadcast_in_dim.2.doc_in
  1.3 0.0 copy-done.1
  1.4 0.0 copy-start
  1.4 0.7 copy.14.q_gain
  2.1 0.0 copy-done.2
  2.1 0.7 copy.15.k_gain
  2.8 0.2 multiply_cosine_fusion.1
  3.0 0.6 pad_maximum_fusion.table_in
  3.6 0.0 copy-done
  3.6 0.8 copy.13
  4.4 149.6 %fused_layer.1 = bf16[4,64,2048]{2,1,0:T(8,128)(2,1)} custom-call(bf16[256,256]{1,0:T(8,128)(2,1)} %bitcast.8, bf16[64,256]{1,0:T(8,128)(2,1)} %bitcast.9, bf16[64,256]{1,0:T(8,128)(2,1)} %bitcast.10, bf16[16,256]{1,0:T(8,128)(2,1)} %broadcast_in_dim.2.doc_in, f32[64,256]{1,0:T(8,128)} %pad_maximum_fusion.table_in, f32[64,1]{1,0:T(8,128)} %copy.14.q_gain, ...), custom_call_target="tpu_custom_call" | custom-call | tf_op jit(solution)/shard_map/fused_layer/pallas_call | solution.py:922
  153.9 2.3 %copy.17 = bf16[256,2048]{1,0:T(8,128)(2,1)} copy(bf16[256,2048]{1,0:T(8,128)(2,1)} %bitcast.7) | data formatting | bytes 2097152
  (3 shorter events, 0.0 us)
Async XLA Ops:
  0.0 0.7 copy-start.3
  0.7 0.7 copy-start.1
  0.7 1.4 copy-start.2
  1.4 2.2 %copy-start = (bf16[256,256]{1,0:T(8,128)(2,1)S(1)}, bf16[256,256]{1,0:T(8,128)(2,1)}, u32[]{:S(2)}) copy-start(bf16[256,256]{1,0:T(8,128)(2,1)} %param.13) | copy-start | bytes 393220

commit v2 on v1

--- a/solution.py
+++ b/solution.py
@@ -269,6 +269,7 @@
 
 SIDES = 2
 LANE = 128
+PIECES = 4
 
 
 def turned(block, gain, table):
@@ -286,6 +287,18 @@
     return jnp.concatenate(pieces, axis=0)
 
 
+def identity(size):
+    down = lax.broadcasted_iota(jnp.int32, (size, size), 0)
+    across = lax.broadcasted_iota(jnp.int32, (size, size), 1)
+    return (down == across).astype(jnp.bfloat16)
+
+
+def flipped(array):
+    return lax.dot_general(
+        identity(array.shape[1]), array, (((1,), (1,)), ((), ())), preferred_element_type=jnp.float32
+    )
+
+
 def fused_kernel(
     n,
     nt,
@@ -294,9 +307,7 @@
     k_in,
     v_in,
     doc_in,
-    table_in,
-    q_gain,
-    k_gain,
+    const_in,
     norm_gain,
     tokens,
     out_weight,
@@ -309,8 +320,10 @@
     top,
     total,
     acc,
-    att_out,
-    att,
+    part,
+    part_in,
+    px_out,
+    px_in,
     ow,
     tok,
     resid,
@@ -336,13 +349,11 @@
     w_ys,
     w_r,
     misc,
-    ow_xs,
-    ow_cs,
-    ow_r,
-    att_s,
-    att_r,
-    act_us,
-    act_ds,
+    pc_s,
+    pc_r,
+    px_s,
+    px_r,
+    act_zs,
     act_xs,
     act_cs,
     act_r,
@@ -358,17 +369,21 @@
 ):
     sp, tp = lax.axis_index("sp"), lax.axis_index("tp")
     lanes, xs = n // SIDES, nt // 2
+    bits = lanes.bit_length() - 1
     lane, side = sp // SIDES, sp % SIDES
     xi, core = tp // 2, tp % 2
-    rows = q_in.shape[1]
+    rows = q_in.shape[0]
     head_dim = k_in.shape[0]
-    heads = q_in.shape[0] // head_dim
+    heads = q_in.shape[1] // head_dim
     chunk = rows // nt
     blocks = gate.shape[1] // LANE
     width = wide * LANE
-    cut = lanes * wide - blocks
+    last = blocks - (lanes - 1) * wide
     kv_docs = head_dim
     kv_vals = kv.shape[1] - head_dim
+    table = const_in[0:head_dim, :]
+    q_gain = const_in[head_dim : 2 * head_dim, :]
+    k_gain = const_in[2 * head_dim : 3 * head_dim, :]
 
     def at_sp(lane_to, side_to):
         return {"sp": lane_to * SIDES + side_to, "tp": tp}
@@ -384,6 +399,12 @@
 
     def x_at(d):
         return (xi + d) % xs
+
+    def bit_of(value, b):
+        return (value // (1 << b)) % 2
+
+    def partner(b):
+        return lane + (1 - 2 * bit_of(lane, b)) * (1 << b)
 
     other_side = 1 - side
     other_core = 1 - core
@@ -392,41 +413,60 @@
     for d in range(1, lanes):
         pl.semaphore_signal(barrier, inc=1, device_id=at_sp(lane_at(d), side), device_id_type=MESH)
     pl.semaphore_signal(barrier, inc=1, device_id=at_sp(lane, other_side), device_id_type=MESH)
-    for d in range(1, nt):
-        pl.semaphore_signal(
-            barrier, inc=1, device_id={"sp": sp, "tp": (tp + d) % nt}, device_id_type=MESH
-        )
-
-    def unit_from(lane_to):
-        return pl.multiple_of((lane_to * wide - (lane_to // (lanes - 1)) * cut) * LANE, LANE)
-
-    def weight_block(m, lane_to):
-        at = pl.ds(unit_from(lane_to), width)
+    for d in range(1, xs):
+        pl.semaphore_signal(barrier, inc=1, device_id=at_tp(x_at(d), core), device_id_type=MESH)
+    pl.semaphore_signal(barrier, inc=1, device_id=at_tp(xi, other_core), device_id_type=MESH)
+
+    def rank(lane_to):
+        return lane_to + core * (lanes - 1 - 2 * lane_to)
+
+    def sized(lane_to, action):
+        if last == wide:
+            action(width)
+            return
+        few = rank(lane_to) // (lanes - 1)
+
+        @pl.when(few == 1)
+        def _():
+            action(last * LANE)
+
+        @pl.when(few == 0)
+        def _():
+            action(width)
+
+    def weight_block(m, lane_to, size):
+        at = pl.ds(pl.multiple_of(rank(lane_to) * width, LANE), size)
         if m == 0:
             return gate.at[:, at]
         if m == 1:
             return up.at[:, at]
         return down.at[at, :]
 
-    landed = (gw, uw, dw)
-
-    own_copies = [
-        pltpu.make_async_copy(weight_block(m, lane), landed[m].at[sp], w_own.at[m]) for m in range(3)
-    ]
-    own_copies.append(pltpu.make_async_copy(out_weight, ow.at[tp], misc.at[0]))
-    own_copies.append(
-        pltpu.make_async_copy(tokens.at[pl.ds(pl.multiple_of(tp * chunk, chunk), chunk)], tok, misc.at[1])
+    def landing(m, slot, size):
+        if m == 0:
+            return gw.at[slot, :, 0:size]
+        if m == 1:
+            return uw.at[slot, :, 0:size]
+        return dw.at[slot, 0:size, :]
+
+    def w_local(m, size):
+        return pltpu.make_async_copy(weight_block(m, lane, size), landing(m, sp, size), w_own.at[m])
+
+    ow_copy = pltpu.make_async_copy(out_weight, ow, misc.at[0])
+    tok_copy = pltpu.make_async_copy(
+        tokens.at[pl.ds(pl.multiple_of(tp * chunk, chunk), chunk)], tok, misc.at[1]
     )
-    for copy in own_copies:
-        copy.start()
-
-    kv[sp, 0:head_dim, :] = turned(k_in[...].astype(jnp.float32), k_gain[...], table_in[...]).astype(
-        jnp.bfloat16
-    )
-    kv[sp, kv_docs:kv_vals, :] = doc_in[...]
+    for m in range(3):
+        sized(lane, lambda size, m=m: w_local(m, size).start())
+    ow_copy.start()
+    tok_copy.start()
+
+    kv[sp, 0:head_dim, :] = turned(k_in[...].astype(jnp.float32), k_gain, table).astype(jnp.bfloat16)
+    q_doc = doc_in[...].astype(jnp.float32)
+    kv[sp, kv_docs:kv_vals, :] = jnp.broadcast_to(q_doc, (kv_vals - kv_docs, rows)).astype(jnp.bfloat16)
     kv[sp, kv_vals:, :] = v_in[...]
 
-    pl.semaphore_wait(barrier, lanes - 1 + 1 + nt - 1)
+    pl.semaphore_wait(barrier, lanes - 1 + 1 + xs - 1 + 1)
 
     def kv_z(d, slot):
         return remote(kv.at[slot], kv.at[slot], kv_zs.at[d], kv_r.at[slot], at_sp(lane_at(d), side))
@@ -441,75 +481,65 @@
         kv_z(d, sp).start()
     kv_y(lane, side).start()
 
-    def ow_x(d):
-        return remote(out_weight, ow.at[tp], ow_xs.at[d], ow_r.at[tp], at_tp(x_at(d), core))
-
-    def ow_core(x_of, core_of):
-        slot = x_of * 2 + core_of
-        return remote(ow.at[slot], ow.at[slot], ow_cs.at[x_of], ow_r.at[slot], at_tp(xi, other_core))
-
-    for d in range(1, xs):
-        ow_x(d).start()
-    own_copies[3].wait()
-    ow_core(xi, core).start()
+    def w_z(m, d, slot, lane_to, size):
+        return remote(
+            weight_block(m, lane_to, size),
+            landing(m, slot, size),
+            w_zs.at[m, d],
+            w_r.at[m, slot],
+            at_sp(lane_at(d), side),
+        )
+
+    def w_y(m, lane_of, side_of, size):
+        slot = lane_of * SIDES + side_of
+        return remote(
+            landing(m, slot, size),
+            landing(m, slot, size),
+            w_ys.at[m, lane_of],
+            w_r.at[m, slot],
+            at_sp(lane, other_side),
+        )
+
+    def start_weight(m):
+        for d in range(1, lanes):
+            lane_to = lane_at(d)
+            sized(lane_to, lambda size, d=d, lane_to=lane_to: w_z(m, d, sp, lane_to, size).start())
+
+        def own(size):
+            w_local(m, size).wait()
+            w_y(m, lane, side, size).start()
+
+        sized(lane, own)
+
+    def w_arrived(m, slot):
+        sized(lane, lambda size: w_z(m, 1, slot, lane, size).wait_recv())
+
+    def w_forward(m, lane_of):
+        sized(lane, lambda size: w_y(m, lane_of, side, size).start())
+
+    def forward_weight(m):
+        for d in range(1, lanes):
+            lane_of = lane_at(lanes - d)
+            w_arrived(m, lane_of * SIDES + side)
+            w_forward(m, lane_of)
 
     scale = head_dim ** (-0.5)
+    standing_q = flipped(q_in[...])
     for h in range(heads):
         at = slice(h * head_dim, (h + 1) * head_dim)
-        query = turned(q_in[at, :].astype(jnp.float32), q_gain[...], table_in[...])
+        query = turned(standing_q[at, :], q_gain, table)
         q_ref[at, :] = (query.astype(jnp.bfloat16).astype(jnp.float32) * scale).astype(jnp.bfloat16)
     top[...] = jnp.full(top.shape, NEG, jnp.float32)
     total[...] = jnp.zeros(total.shape, jnp.float32)
     acc[...] = jnp.zeros(acc.shape, jnp.float32)
 
-    for d in range(1, lanes):
-        slot = lane_at(-d) * SIDES + side
-        kv_z(d, slot).wait_recv()
-        kv_y(lane_at(-d), side).start()
-
-    def w_z(m, d, slot):
-        return remote(
-            weight_block(m, lane_at(d)),
-            landed[m].at[slot],
-            w_zs.at[m, d],
-            w_r.at[m, slot],
-            at_sp(lane_at(d), side),
-        )
-
-    def w_y(m, lane_of, side_of):
-        slot = lane_of * SIDES + side_of
-        return remote(
-            landed[m].at[slot],
-            landed[m].at[slot],
-            w_ys.at[m, lane_of],
-            w_r.at[m, slot],
-            at_sp(lane, other_side),
-        )
-
-    for m in range(3):
-        for d in range(1, lanes):
-            w_z(m, d, sp).start()
-        own_copies[m].wait()
-        w_y(m, lane, side).start()
-
-    eye = (
-        lax.broadcasted_iota(jnp.int32, (rows, rows), 0)
-        == lax.broadcasted_iota(jnp.int32, (rows, rows), 1)
-    ).astype(jnp.bfloat16)
-    across = (((1,), (1,)), ((), ()))
-    q_doc = doc_in[0:1, :].astype(jnp.float32)
-
-    @pl.loop(0, n)
-    def _(k):
-        lane_of = (lane + k) % lanes
-        side_of = (side + k // lanes) % SIDES
-        slot = lane_of * SIDES + side_of
-
-        @pl.when(k >= lanes)
-        def _():
-            kv_y(lane_of, side_of).wait_recv()
-
-        upright = lax.dot_general(eye, kv[slot, 0:kv_vals, :], across, preferred_element_type=jnp.float32)
+    def absorb(slot):
+        upright = lax.dot_general(
+            identity(rows),
+            kv[slot, 0:kv_vals, :],
+            (((1,), (1,)), ((), ())),
+            preferred_element_type=jnp.float32,
+        )
         key = upright[:, 0:head_dim].astype(jnp.bfloat16)
         same = upright[:, head_dim : head_dim + 1] == q_doc
         value = kv[slot, kv_vals:, :]
@@ -527,70 +557,94 @@
                 value, weights.astype(jnp.bfloat16), preferred_element_type=jnp.float32
             )
 
+    @pl.loop(0, SIDES)
+    def _(k):
+        side_of = (side + k) % SIDES
+
+        @pl.when(k > 0)
+        def _():
+            kv_y(lane, other_side).wait_recv()
+
+        absorb(lane * SIDES + side_of)
+
+    @pl.loop(0, SIDES * (lanes - 1))
+    def _(k):
+        lane_of = lane_at(k % (lanes - 1) + 1)
+        side_of = (side + k // (lanes - 1)) % SIDES
+        slot = lane_of * SIDES + side_of
+
+        @pl.when(k < lanes - 1)
+        def _():
+            kv_z(1, slot).wait_recv()
+            kv_y(lane_of, side).start()
+
+        @pl.when(k == lanes - 2)
+        def _():
+            start_weight(0)
+            start_weight(1)
+
+        @pl.when(k >= lanes - 1)
+        def _():
+            kv_y(lane_of, other_side).wait_recv()
+
+        absorb(slot)
+
     pieces = []
     for h in range(heads):
         at = slice(h * head_dim, (h + 1) * head_dim)
         pieces.append((acc[at, :] / total[h]).astype(jnp.bfloat16))
-    standing = jnp.concatenate(pieces, axis=0)
-    attended = lax.dot_general(eye, standing, across, preferred_element_type=jnp.float32).astype(
-        jnp.bfloat16
-    )
-    for i in range(nt):
-        att_out[i] = attended[i * chunk : (i + 1) * chunk]
-
-    def att_copy(d, peer, slot):
-        return remote(
-            att_out.at[peer], att.at[slot], att_s.at[d], att_r.at[slot], {"sp": sp, "tp": peer}
-        )
-
-    for d in range(1, nt):
-        att_copy(d, (tp + d) % nt, tp).start()
-    att[tp] = att_out[tp]
-
-    def project(slot):
-        return (
-            jnp.dot(att[slot], ow[slot], preferred_element_type=jnp.float32)
-            .astype(jnp.bfloat16)
-            .astype(jnp.float32)
-        )
-
-    own_copies[4].wait()
-    resid[...] = tok[...].astype(jnp.float32) + project(tp)
-    for d in range(1, nt):
-        slot = (tp + nt - d) % nt
-        att_copy(d, tp, slot).wait_recv()
-    ow_core(xi, other_core).wait_recv()
-    resid[...] += project(xi * 2 + other_core)
-    for d in range(1, xs):
-        x_of = x_at(xs - d)
-        remote(out_weight, ow.at[x_of * 2 + core], ow_xs.at[d], ow_r.at[x_of * 2 + core], at_tp(x_of, core)).wait_recv()
-        ow_core(x_of, core).start()
-        resid[...] += project(x_of * 2 + core)
-    for d in range(1, xs):
-        x_of = x_at(xs - d)
-        ow_core(x_of, other_core).wait_recv()
-        resid[...] += project(x_of * 2 + other_core)
+    attended = flipped(jnp.concatenate(pieces, axis=0)).astype(jnp.bfloat16)
+
+    span = ow.shape[1] // PIECES
+
+    def part_core(p):
+        return remote(part.at[p, other_core], part_in.at[p], pc_s.at[p], pc_r.at[p], at_tp(xi, other_core))
+
+    def part_x(p, d):
+        return remote(px_out.at[p, d], px_in.at[p, d], px_s.at[p, d], px_r.at[p, d], at_tp(x_at(d), core))
+
+    ow_copy.wait()
+    for p in range(PIECES):
+        product = jnp.dot(
+            attended, ow[:, p * span : (p + 1) * span], preferred_element_type=jnp.float32
+        ).astype(jnp.bfloat16)
+        for x_of in range(xs):
+            for core_of in range(2):
+                start = (x_of * 2 + core_of) * chunk
+                part[p, core_of, x_of] = product[start : start + chunk]
+        part_core(p).start()
+    tok_copy.wait()
+    for p in range(PIECES):
+        at = slice(p * span, (p + 1) * span)
+        part_core(p).wait_recv()
+        for d in range(1, xs):
+            x_to = x_at(d)
+            px_out[p, d] = (
+                part[p, core, x_to].astype(jnp.float32) + part_in[p, x_to].astype(jnp.float32)
+            ).astype(jnp.bfloat16)
+            part_x(p, d).start()
+        resid[:, at] = (
+            tok[:, at].astype(jnp.float32)
+            + part[p, core, xi].astype(jnp.float32)
+            + part_in[p, xi].astype(jnp.float32)
+        )
+    for p in range(PIECES):
+        at = slice(p * span, (p + 1) * span)
+        for d in range(1, xs):
+            part_x(p, d).wait_recv()
+            resid[:, at] += px_in[p, d].astype(jnp.float32)
 
     whole = resid[...]
     power = jnp.mean(whole * whole, axis=-1, keepdims=True)
     act[lane, tp] = (whole * lax.rsqrt(power + EPS) * norm_gain[...]).astype(jnp.bfloat16)
 
-    def act_up(lane_of):
+    def act_z(b, lane_of):
         return remote(
             act.at[lane_of, tp],
             act.at[lane_of, tp],
-            act_us.at[lane_of],
+            act_zs.at[b, lane_of],
             act_r.at[lane_of, tp],
-            at_sp(lane + 1, side),
-        )
-
-    def act_down(lane_of):
-        return remote(
-            act.at[lane_of, tp],
-            act.at[lane_of, tp],
-            act_ds.at[lane_of],
-            act_r.at[lane_of, tp],
-            at_sp(lane - 1, side),
+            at_sp(partner(b), side),
         )
 
     def act_x(d, lane_of, slot):
@@ -623,73 +677,50 @@
             act_x(d, lane_of, x_of * 2 + core).wait_recv()
             act_core(lane_of, x_of, core).start()
 
-    rises, falls = lane < lanes - 1, lane > 0
-
-    @pl.when(rises)
-    def _():
-        act_up(lane).start()
-
-    @pl.when(falls)
-    def _():
-        act_down(lane).start()
-
+    for b in reversed(range(bits)):
+        act_z(b, lane).start()
     act_out(lane)
-
-    def forward_weight(m):
-        for d in range(1, lanes):
-            lane_of = lane_at(lanes - d)
-            w_z(m, d, lane_of * SIDES + side).wait_recv()
-            w_y(m, lane_of, side).start()
-
     forward_weight(0)
-    for d in range(1, lanes):
-
-        @pl.when(lane >= d)
-        def _():
-            act_up(lane - d).wait_recv()
-
-            @pl.when(rises)
-            def _():
-                act_up(lane - d).start()
-
-            act_out(lane - d)
-
-        @pl.when(lane + d < lanes)
-        def _():
-            act_down(lane + d).wait_recv()
-
-            @pl.when(falls)
-            def _():
-                act_down(lane + d).start()
-
-            act_out(lane + d)
-
-        if d == 1:
-            act_from_x(lane)
+    act_from_x(lane)
     forward_weight(1)
-    for d in range(1, lanes):
-
-        @pl.when(lane >= d)
-        def _():
-            act_from_x(lane - d)
-
-        @pl.when(lane + d < lanes)
-        def _():
-            act_from_x(lane + d)
+    for b in reversed(range(bits)):
+        if b == 0:
+            start_weight(2)
+        mate = partner(b)
+        count = lanes >> (b + 1)
+        for i in range(count):
+            turn = (mate // (1 << (b + 1)) + i) % count
+            lane_of = mate % (1 << (b + 1)) + turn * (1 << (b + 1))
+            act_z(b, lane_of).wait_recv()
+            for lower in reversed(range(b)):
+                act_z(lower, lane_of).start()
+            act_out(lane_of)
 
     for m in range(2):
         for d in range(lanes):
-            w_y(m, lane_at(d), other_side).wait_recv()
-
+            sized(lane, lambda size, m=m, d=d: w_y(m, lane_at(d), other_side, size).wait_recv())
+
+    few_here = rank(lane) // (lanes - 1)
     unit = lax.broadcasted_iota(jnp.int32, (nt * chunk, width), 1)
-    mine = unit >= (lane // (lanes - 1)) * cut * LANE
-    for d in range(lanes):
-        lane_of = lane_at(d)
+    mine = unit < (wide - few_here * (wide - last)) * LANE
+    if last < wide:
+
+        @pl.when(few_here == 1)
+        def _():
+            dw[:, last * LANE :, :] = jnp.zeros((n, width - last * LANE, dw.shape[2]), dw.dtype)
+
+    @pl.loop(0, lanes)
+    def _(i):
+        lane_of = 0
+        for b in range(bits):
+            lane_of = lane_of + (bit_of(lane, b) + bit_of(i, bits - 1 - b)) % 2 * (1 << b)
+
+        @pl.when(i > 0)
+        def _():
+            act_from_x(lane_of)
+
         for x_of in range(xs):
             act_core(lane_of, x_of, other_core).wait_recv()
-
-    @pl.loop(0, lanes)
-    def _(lane_of):
         inputs = act[lane_of].reshape(nt * chunk, act.shape[-1])
         gated = jnp.dot(inputs, gw[...].reshape(n * gw.shape[1], width), preferred_element_type=jnp.float32)
         lifted = jnp.dot(inputs, uw[...].reshape(n * uw.shape[1], width), preferred_element_type=jnp.float32)
@@ -702,6 +733,7 @@
 
     cols = dw.shape[2]
     share = xs * lanes * chunk
+    starts = [lanes - (lanes >> b) for b in range(bits)]
 
     def rs_core(s):
         return remote(core_out.at[s], core_in.at[s], rs_cs.at[s], rs_cr.at[s], at_tp(xi, other_core))
@@ -709,9 +741,10 @@
     def rs_x(s, d):
         return remote(x_out.at[s, d], x_in.at[s, d], rs_xs.at[s, d], rs_xr.at[s, d], at_tp(x_at(d), core))
 
-    def rs_z(s, d):
+    def rs_z(s, b):
+        piece = pl.ds(starts[b], lanes >> (b + 1))
         return remote(
-            z_out.at[s, d], z_in.at[s, d], rs_zs.at[s, d], rs_zr.at[s, d], at_sp(lane_at(d), side)
+            z_out.at[s, piece], z_in.at[s, piece], rs_zs.at[s, b], rs_zr.at[s, b], at_sp(partner(b), side)
         )
 
     def columns(s):
@@ -727,84 +760,95 @@
         return remote(piece, piece, ag_cs.at[s, x_of], ag_r.at[s, slot], at_tp(xi, other_core))
 
     def slot_of(k):
-        return (k // SIDES) * SIDES + (side + k) % SIDES
-
-    @pl.loop(0, n + 4)
-    def _(k):
-        @pl.when(k < n)
+        j = k // SIDES
+        lane_of = lanes // 2 + (1 - 2 * (j % 2)) * (j // 2) - j % 2
+        return lane_of * SIDES + (side + k) % SIDES
+
+    def multiply(k):
+        s = slot_of(k)
+        lane_of, side_of = s // SIDES, s % SIDES
+
+        @pl.when(side_of == side)
         def _():
-            s = slot_of(k)
-            lane_of, side_of = s // SIDES, s % SIDES
-
-            @pl.when(side_of == side)
+            @pl.when(lane_of != lane)
             def _():
-                @pl.when(lane_of != lane)
-                def _():
-                    w_z(2, 1, s).wait_recv()
-                    w_y(2, lane_of, side).start()
-
-            @pl.when(side_of != side)
-            def _():
-                w_y(2, lane_of, other_side).wait_recv()
-
-            away = hid[other_core].reshape(share, width)
-            core_out[s] = (
-                jnp.dot(away, dw[s], preferred_element_type=jnp.float32)
-                .astype(jnp.bfloat16)
-                .reshape(xs, lanes, chunk, cols)
-            )
-            rs_core(s).start()
-            near = hid[core].reshape(share, width)
-            keep[s] = jnp.dot(near, dw[s], preferred_element_type=jnp.float32).reshape(
-                xs, lanes, chunk, cols
-            )
-
-        @pl.when((k >= 1) & (k < n + 1))
+                w_arrived(2, s)
+                w_forward(2, lane_of)
+
+        @pl.when(side_of != side)
         def _():
-            s = slot_of(k - 1)
-            rs_core(s).wait_recv()
-            for d in range(1, xs):
-                x_to = x_at(d)
-                x_out[s, d] = (keep[s, x_to] + core_in[s, x_to].astype(jnp.float32)).astype(jnp.bfloat16)
-                rs_x(s, d).start()
-            x_keep[s] = keep[s, xi] + core_in[s, xi].astype(jnp.float32)
-
-        @pl.when((k >= 2) & (k < n + 2))
-        def _():
-            s = slot_of(k - 2)
+            sized(lane, lambda size: w_y(2, lane_of, other_side, size).wait_recv())
+
+        away = hid[other_core].reshape(share, width)
+        core_out[s] = (
+            jnp.dot(away, dw[s], preferred_element_type=jnp.float32)
+            .astype(jnp.bfloat16)
+            .reshape(xs, lanes, chunk, cols)
+        )
+        rs_core(s).start()
+        near = hid[core].reshape(share, width)
+        keep[s] = jnp.dot(near, dw[s], preferred_element_type=jnp.float32).reshape(xs, lanes, chunk, cols)
+
+    def reduce_core(k):
+        s = slot_of(k)
+        rs_core(s).wait_recv()
+        for d in range(1, xs):
+            x_to = x_at(d)
+            x_out[s, d] = (keep[s, x_to] + core_in[s, x_to].astype(jnp.float32)).astype(jnp.bfloat16)
+            rs_x(s, d).start()
+        x_keep[s] = keep[s, xi] + core_in[s, xi].astype(jnp.float32)
+
+    def reduce_lanes(b, k):
+        s = slot_of(k)
+        if b == 0:
             for d in range(1, xs):
                 rs_x(s, d).wait_recv()
-
-            def summed(lane_to):
-                value = x_keep[s, lane_to]
+        else:
+            rs_z(s, b - 1).wait_recv()
+
+        def summed(h):
+            if b == 0:
+                value = x_keep[s, h]
                 for d in range(1, xs):
-                    value = value + x_in[s, d, lane_to].astype(jnp.float32)
+                    value = value + x_in[s, d, h].astype(jnp.float32)
                 return value
-
-            for d in range(1, lanes):
-                z_out[s, d] = summed(lane_at(d)).astype(jnp.bfloat16)
-                rs_z(s, d).start()
-            z_keep[s] = summed(lane)
-
-        @pl.when((k >= 3) & (k < n + 3))
-        def _():
-            s = slot_of(k - 3)
-            value = z_keep[s]
-            for d in range(1, lanes):
-                rs_z(s, d).wait_recv()
-                value = value + z_in[s, d].astype(jnp.float32)
-            out[tp, :, columns(s)] = (resid[:, columns(s)] + value).astype(jnp.bfloat16)
+            return z_keep[b - 1, s, h] + z_in[s, starts[b - 1] + h].astype(jnp.float32)
+
+        if b == bits:
+            out[tp, :, columns(s)] = (resid[:, columns(s)] + summed(0)).astype(jnp.bfloat16)
             for d in range(1, xs):
                 ag_x(s, d, tp).start()
             ag_core(s, xi, core).start()
-
-        @pl.when(k >= 4)
-        def _():
-            s = slot_of(k - 4)
-            for d in range(1, xs):
-                x_of = x_at(xs - d)
-                ag_x(s, d, x_of * 2 + core).wait_recv()
-                ag_core(s, x_of, core).start()
+            return
+        mine_here = bit_of(lane, b)
+        count = lanes >> (b + 1)
+        for h in range(count):
+            z_out[s, starts[b] + h] = summed(1 - mine_here + 2 * h).astype(jnp.bfloat16)
+        rs_z(s, b).start()
+        for h in range(count):
+            z_keep[b, s, h] = summed(mine_here + 2 * h)
+
+    def spread(k):
+        s = slot_of(k)
+        for d in range(1, xs):
+            x_of = x_at(xs - d)
+            ag_x(s, d, x_of * 2 + core).wait_recv()
+            ag_core(s, x_of, core).start()
+
+    stages = [(0, multiply), (1, reduce_core)]
+    at = 3
+    for b in range(bits + 1):
+        stages.append((at, functools.partial(reduce_lanes, b)))
+        at += 2
+    stages.append((at, spread))
+
+    @pl.loop(0, n + at)
+    def _(k):
+        for lag, action in reversed(stages):
+
+            @pl.when((k >= lag) & (k < n + lag))
+            def _(lag=lag, action=action):
+                action(k - lag)
 
     @pl.loop(0, n)
     def _(s):
@@ -815,52 +859,47 @@
             ag_x(s, d, tp).wait_send()
             rs_x(s, d).wait_send()
         rs_core(s).wait_send()
-        for d in range(1, lanes):
-            rs_z(s, d).wait_send()
+        for b in range(bits):
+            rs_z(s, b).wait_send()
 
     for d in range(1, lanes):
         kv_z(d, sp).wait_send()
         for m in range(3):
-            w_z(m, d, sp).wait_send()
+            lane_to = lane_at(d)
+            sized(lane_to, lambda size, m=m, d=d, lane_to=lane_to: w_z(m, d, sp, lane_to, size).wait_send())
     for lane_of in range(lanes):
         kv_y(lane_of, side).wait_send()
         for m in range(3):
-            w_y(m, lane_of, side).wait_send()
+            sized(lane, lambda size, m=m, lane_of=lane_of: w_y(m, lane_of, side, size).wait_send())
         for d in range(1, xs):
             act_x(d, lane_of, tp).wait_send()
         for x_of in range(xs):
             act_core(lane_of, x_of, core).wait_send()
-
-        @pl.when(rises & (lane_of <= lane))
-        def _():
-            act_up(lane_of).wait_send()
-
-        @pl.when(falls & (lane_of >= lane))
-        def _():
-            act_down(lane_of).wait_send()
-
-    for d in range(1, xs):
-        ow_x(d).wait_send()
-    for x_of in range(xs):
-        ow_core(x_of, core).wait_send()
-    for d in range(1, nt):
-        att_copy(d, (tp + d) % nt, tp).wait_send()
+    for b in range(bits):
+        for h in range(lanes >> (b + 1)):
+            act_z(b, lane % (1 << (b + 1)) + h * (1 << (b + 1))).wait_send()
+    for p in range(PIECES):
+        part_core(p).wait_send()
+        for d in range(1, xs):
+            part_x(p, d).wait_send()
 
 
 VMEM_LIMIT = 60 * 1024 * 1024
 
 
 def fused_plan(n, nt, rows, width, head_dim, heads, units):
-    if n % SIDES or n < 2 * SIDES or nt % 2 or rows % nt or units % LANE:
+    if n % SIDES or n < 2 * SIDES or nt % 2 or nt < 4 or rows % nt or units % LANE:
         return None
     lanes, xs, chunk, blocks = n // SIDES, nt // 2, rows // nt, units // LANE
     wide = -(-blocks // lanes)
     cols = width // n
-    if chunk % 16 or rows % LANE or cols % LANE or width % n or head_dim % 32:
+    if chunk % 16 or rows % LANE or width % (n * LANE) or width % (PIECES * LANE) or head_dim % 64:
         return None
-    if wide > blocks or (lanes - 1) * wide > blocks:
+    if lanes & (lanes - 1) or (lanes - 1) * wide >= blocks:
         return None
     wu = wide * LANE
+    bits = lanes.bit_length() - 1
+    span = width // PIECES
     bf, f32 = jnp.bfloat16, jnp.float32
     shapes = [
         ((n, 2 * head_dim + 16, rows), bf),
@@ -868,14 +907,16 @@
         ((heads, 1, rows), f32),
         ((heads, 1, rows), f32),
         ((heads * head_dim, rows), f32),
-        ((nt, chunk, heads * head_dim), bf),
-        ((nt, chunk, heads * head_dim), bf),
-        ((nt, heads * head_dim, width), bf),
+        ((PIECES, 2, xs, chunk, span), bf),
+        ((PIECES, xs, chunk, span), bf),
+        ((PIECES, xs, chunk, span), bf),
+        ((PIECES, xs, chunk, span), bf),
+        ((heads * head_dim, width), bf),
         ((chunk, width), bf),
         ((chunk, width), f32),
         ((lanes, nt, chunk, width), bf),
-        ((n, width // n, wu), bf),
-        ((n, width // n, wu), bf),
+        ((n, cols, wu), bf),
+        ((n, cols, wu), bf),
         ((n, wu, cols), bf),
         ((2, xs, lanes, chunk, wu), bf),
         ((n, xs, lanes, chunk, cols), f32),
@@ -884,9 +925,9 @@
         ((n, lanes, chunk, cols), f32),
         ((n, xs, lanes, chunk, cols), bf),
         ((n, xs, lanes, chunk, cols), bf),
-        ((n, chunk, cols), f32),
-        ((n, lanes, chunk, cols), bf),
-        ((n, lanes, chunk, cols), bf),
+        ((bits, n, lanes // 2, chunk, cols), f32),
+        ((n, lanes - 1, chunk, cols), bf),
+        ((n, lanes - 1, chunk, cols), bf),
     ]
     size = 0
     for shape, kind in shapes:
@@ -897,9 +938,9 @@
     if size > VMEM_LIMIT * 3 // 4:
         return None
     sems = [(lanes,), (lanes,), (n,), (3,), (3, lanes), (3, lanes), (3, n), (2,)]
-    sems += [(xs,), (xs,), (nt,), (nt,), (nt,)]
-    sems += [(lanes,), (lanes,), (xs, lanes), (lanes, xs), (lanes, nt)]
-    sems += [(n,), (n,), (n, xs), (n, xs), (n, lanes), (n, lanes), (n, xs), (n, xs), (n, nt)]
+    sems += [(PIECES,), (PIECES,), (PIECES, xs), (PIECES, xs)]
+    sems += [(bits, lanes), (xs, lanes), (lanes, xs), (lanes, nt)]
+    sems += [(n,), (n,), (n, xs), (n, xs), (n, bits), (n, bits), (n, xs), (n, xs), (n, nt)]
     return wide, [pltpu.VMEM(*s) for s in shapes] + [pltpu.SemaphoreType.DMA(s) for s in sems]
 
 
@@ -916,13 +957,13 @@
     angles = [
         freqs[:, None] * spot.astype(jnp.float32)[None, :] for spot in (places // GRID, places % GRID)
     ]
-    table = jnp.concatenate([f(a) for a in angles for f in (jnp.cos, jnp.sin)], axis=0)
-    docs = jnp.broadcast_to(doc_ids.astype(jnp.bfloat16)[None, :], (16, rows))
+    consts = [f(a) for a in angles for f in (jnp.cos, jnp.sin)]
+    consts += [jnp.broadcast_to(g[:, None], (head_dim, rows)) for g in (query_gain, key_norm_scale)]
     hbm = pl.BlockSpec(memory_space=pl.ANY)
     out = pl.pallas_call(
         functools.partial(fused_kernel, n, nt, wide),
         out_shape=jax.ShapeDtypeStruct((nt, rows // nt, width), jnp.bfloat16),
-        in_specs=[VM] * 8 + [hbm] * 5,
+        in_specs=[VM] * 6 + [hbm] * 5,
         out_specs=VM,
         scratch_shapes=scratch,
         compiler_params=pltpu.CompilerParams(
@@ -930,9 +971,8 @@
         ),
         name="fused_layer",
     )(
-        queries.T, keys.T, values.T, docs, table,
-        query_gain.reshape(head_dim, 1), key_norm_scale.reshape(head_dim, 1), norm_gain.reshape(1, width),
-        tokens_in, out_weight, gate_weight, up_weight, down_weight,
+        queries, keys.T, values.T, doc_ids.reshape(1, rows), jnp.concatenate(consts, axis=0),
+        norm_gain.reshape(1, width), tokens_in, out_weight, gate_weight, up_weight, down_weight,
     )
     return out.reshape(rows, width)
 

time: 156 us -> 132 us (0.85)
  Pallas kernels: 150 us -> 127 us
  local copies, waits for them, and re-layouts: 5.79 us -> 4.22 us
    pallas_call x1, Pallas kernels: 150 us -> 127 us  [fused_layer(): pl.pallas_call(functools.partial(fused_kernel, n, nt, wide), out_shape=ja...]
    unnamed x10 -> x8, local copies, waits for them, and re-layouts: 3.79 us -> 4.15 us
where the time goes in v2:
time: 132 us
  Pallas kernels  127 us (96%)
  local copies, waits for them, and re-layouts  4.22 us (3%)
    pallas_call x1, Pallas kernels, fused_layer(): pl.pallas_call(functools.partial(fused_kernel, n, nt, wide), out_shape=ja...  127 us
    unnamed x8, local copies, waits for them, and re-layouts  4.15 us

profile of v2, /device:TPU:0, one launch (start us, length us, event | category | flops | bytes accessed | tf_op | source)
XLA Modules:
  0.0 132.0 jit_solution(11359303539040745848)
XLA Ops:
  0.0 0.1 fusion
  0.2 0.1 fusion.1
  0.3 0.1 fusion.2
  0.5 0.0 copy-start.1
  0.5 0.1 fusion.3
  0.6 0.5 copy-done.1
  1.1 0.0 copy-start.2
  1.1 0.1 broadcast_dynamic-update-slice_fusion.1
  1.2 0.6 copy-done.2
  1.8 0.1 broadcast_dynamic-update-slice_fusion.const_in
  1.8 0.0 copy-start
  1.8 0.7 copy-done
  2.5 127.2 %fused_layer.1 = bf16[4,64,2048]{2,1,0:T(8,128)(2,1)} custom-call(bf16[256,256]{1,0:T(8,128)(2,1)} %q_in.1, bf16[64,256]{1,0:T(8,128)(2,1)} %bitcast.6, bf16[64,256]{1,0:T(8,128)(2,1)} %bitcast.7, s32[1,256]{1,0:T(1,128)} %bitcast.9, f32[192,256]{1,0:T(8,128)} %copy-done, f32[1,2048]{1,0:T(1,128)} %bitcast.8, bf16[256,2048]{1,0:T(8,128)(2,1)} %tokens.1, ...), custom_call_target="tpu_custom_call" | custom-call | tf_op jit(solution)/shard_map/fused_layer/pallas_call | solution.py:963
  129.7 2.3 %copy.19 = bf16[256,2048]{1,0:T(8,128)(2,1)} copy(bf16[256,2048]{1,0:T(8,128)(2,1)} %bitcast.5) | data formatting | bytes 2097152
  (2 shorter events, 0.0 us)
Async XLA Ops:
  0.5 0.7 copy-start.1
  1.1 0.7 copy-start.2
  1.8 0.7 copy-start

commit v3 on v2

--- a/solution.py
+++ b/solution.py
@@ -299,6 +299,13 @@
     )
 
 
+def upright_row(row):
+    size = row.shape[1]
+    down = lax.broadcasted_iota(jnp.int32, (size, size), 0)
+    across = lax.broadcasted_iota(jnp.int32, (size, size), 1)
+    return jnp.sum(jnp.where(down == across, row, 0.0), axis=1, keepdims=True)
+
+
 def fused_kernel(
     n,
     nt,
@@ -307,14 +314,22 @@
     k_in,
     v_in,
     doc_in,
-    const_in,
-    norm_gain,
+    q_gain_in,
+    k_gain_in,
+    norm_gain_in,
     tokens,
     out_weight,
     gate,
     up,
     down,
+    table_ref,
     out,
+    q_raw,
+    k_raw,
+    doc_ref,
+    q_gain_ref,
+    k_gain_ref,
+    norm_gain,
     kv,
     q_ref,
     top,
@@ -331,6 +346,7 @@
     gw,
     uw,
     dw,
+    gated,
     hid,
     keep,
     core_out,
@@ -380,10 +396,7 @@
     width = wide * LANE
     last = blocks - (lanes - 1) * wide
     kv_docs = head_dim
-    kv_vals = kv.shape[1] - head_dim
-    table = const_in[0:head_dim, :]
-    q_gain = const_in[head_dim : 2 * head_dim, :]
-    k_gain = const_in[2 * head_dim : 3 * head_dim, :]
+    table = table_ref[...]
 
     def at_sp(lane_to, side_to):
         return {"sp": lane_to * SIDES + side_to, "tp": tp}
@@ -405,6 +418,18 @@
 
     def partner(b):
         return lane + (1 - 2 * bit_of(lane, b)) * (1 << b)
+
+    def mate(e):
+        return lane + sum((e >> b) % 2 * (1 - 2 * bit_of(lane, b)) * (1 << b) for b in range(bits))
+
+    def mated(i):
+        total_of = 0
+        for b in range(bits):
+            total_of = total_of + (bit_of(lane, b) + bit_of(i, b)) % 2 * (1 << b)
+        return total_of
+
+    def low_bit(e):
+        return (e & -e).bit_length() - 1
 
     other_side = 1 - side
     other_core = 1 - core
@@ -456,20 +481,35 @@
     tok_copy = pltpu.make_async_copy(
         tokens.at[pl.ds(pl.multiple_of(tp * chunk, chunk), chunk)], tok, misc.at[1]
     )
+    kv_vals = kv.shape[1] - head_dim
+    small = [
+        pltpu.make_async_copy(k_in, k_raw, misc.at[2]),
+        pltpu.make_async_copy(doc_in, doc_ref, misc.at[3]),
+        pltpu.make_async_copy(k_gain_in, k_gain_ref, misc.at[4]),
+        pltpu.make_async_copy(v_in, kv.at[sp, kv_vals:, :], misc.at[5]),
+        pltpu.make_async_copy(q_in, q_raw, misc.at[6]),
+        pltpu.make_async_copy(q_gain_in, q_gain_ref, misc.at[7]),
+        pltpu.make_async_copy(norm_gain_in, norm_gain, misc.at[8]),
+    ]
+    for copy in small:
+        copy.start()
     for m in range(3):
         sized(lane, lambda size, m=m: w_local(m, size).start())
     ow_copy.start()
     tok_copy.start()
 
-    kv[sp, 0:head_dim, :] = turned(k_in[...].astype(jnp.float32), k_gain, table).astype(jnp.bfloat16)
-    q_doc = doc_in[...].astype(jnp.float32)
+    for copy in small[:4]:
+        copy.wait()
+    k_full = turned(k_raw[...].astype(jnp.float32), upright_row(k_gain_ref[...]), table)
+    kv[sp, 0:head_dim, :] = k_full.astype(jnp.bfloat16)
+    q_doc = doc_ref[...].astype(jnp.float32)
     kv[sp, kv_docs:kv_vals, :] = jnp.broadcast_to(q_doc, (kv_vals - kv_docs, rows)).astype(jnp.bfloat16)
-    kv[sp, kv_vals:, :] = v_in[...]
 
     pl.semaphore_wait(barrier, lanes - 1 + 1 + xs - 1 + 1)
 
-    def kv_z(d, slot):
-        return remote(kv.at[slot], kv.at[slot], kv_zs.at[d], kv_r.at[slot], at_sp(lane_at(d), side))
+    def kv_z(e, lane_of):
+        slot = lane_of * SIDES + side
+        return remote(kv.at[slot], kv.at[slot], kv_zs.at[e], kv_r.at[slot], at_sp(mate(e), side))
 
     def kv_y(lane_of, side_of):
         slot = lane_of * SIDES + side_of
@@ -477,17 +517,17 @@
             kv.at[slot], kv.at[slot], kv_ys.at[lane_of], kv_r.at[slot], at_sp(lane, other_side)
         )
 
-    for d in range(1, lanes):
-        kv_z(d, sp).start()
+    for e in range(1, lanes):
+        kv_z(e, lane).start()
     kv_y(lane, side).start()
 
-    def w_z(m, d, slot, lane_to, size):
+    def w_z(m, e, slot, lane_to, size):
         return remote(
             weight_block(m, lane_to, size),
             landing(m, slot, size),
-            w_zs.at[m, d],
+            w_zs.at[m, e],
             w_r.at[m, slot],
-            at_sp(lane_at(d), side),
+            at_sp(mate(e), side),
         )
 
     def w_y(m, lane_of, side_of, size):
@@ -500,31 +540,33 @@
             at_sp(lane, other_side),
         )
 
-    def start_weight(m):
-        for d in range(1, lanes):
-            lane_to = lane_at(d)
-            sized(lane_to, lambda size, d=d, lane_to=lane_to: w_z(m, d, sp, lane_to, size).start())
-
+    def send_weight(m, e):
+        lane_to = mate(e)
+        sized(lane_to, lambda size: w_z(m, e, sp, lane_to, size).start())
+
+    def share_weight(m):
         def own(size):
             w_local(m, size).wait()
             w_y(m, lane, side, size).start()
 
         sized(lane, own)
 
-    def w_arrived(m, slot):
-        sized(lane, lambda size: w_z(m, 1, slot, lane, size).wait_recv())
-
-    def w_forward(m, lane_of):
+    def forward_weight(m, lane_of):
+        sized(lane, lambda size: w_z(m, 1, lane_of * SIDES + side, lane, size).wait_recv())
         sized(lane, lambda size: w_y(m, lane_of, side, size).start())
 
-    def forward_weight(m):
-        for d in range(1, lanes):
-            lane_of = lane_at(lanes - d)
-            w_arrived(m, lane_of * SIDES + side)
-            w_forward(m, lane_of)
+    def w_shared(m, lane_of):
+        sized(lane, lambda size: w_y(m, lane_of, other_side, size).wait_recv())
+
+    for e in range(1, lanes):
+        send_weight(0, e)
+    share_weight(0)
 
     scale = head_dim ** (-0.5)
-    standing_q = flipped(q_in[...])
+    for copy in small[4:]:
+        copy.wait()
+    standing_q = flipped(q_raw[...])
+    q_gain = upright_row(q_gain_ref[...])
     for h in range(heads):
         at = slice(h * head_dim, (h + 1) * head_dim)
         query = turned(standing_q[at, :], q_gain, table)
@@ -569,19 +611,14 @@
 
     @pl.loop(0, SIDES * (lanes - 1))
     def _(k):
-        lane_of = lane_at(k % (lanes - 1) + 1)
+        lane_of = mated(k % (lanes - 1) + 1)
         side_of = (side + k // (lanes - 1)) % SIDES
         slot = lane_of * SIDES + side_of
 
         @pl.when(k < lanes - 1)
         def _():
-            kv_z(1, slot).wait_recv()
+            kv_z(1, lane_of).wait_recv()
             kv_y(lane_of, side).start()
-
-        @pl.when(k == lanes - 2)
-        def _():
-            start_weight(0)
-            start_weight(1)
 
         @pl.when(k >= lanes - 1)
         def _():
@@ -589,6 +626,8 @@
 
         absorb(slot)
 
+    send_weight(1, 1)
+    share_weight(1)
     pieces = []
     for h in range(heads):
         at = slice(h * head_dim, (h + 1) * head_dim)
@@ -677,28 +716,26 @@
             act_x(d, lane_of, x_of * 2 + core).wait_recv()
             act_core(lane_of, x_of, core).start()
 
+    def act_arrived(e):
+        step = low_bit(e)
+        act_z(step, mate(e)).wait_recv()
+        for lower in reversed(range(step)):
+            act_z(lower, mate(e)).start()
+        act_out(mate(e))
+
     for b in reversed(range(bits)):
         act_z(b, lane).start()
     act_out(lane)
-    forward_weight(0)
+    for e in range(2, lanes - 1):
+        send_weight(1, e)
+    for e in range(1, lanes):
+        forward_weight(0, mate(e))
     act_from_x(lane)
-    forward_weight(1)
-    for b in reversed(range(bits)):
-        if b == 0:
-            start_weight(2)
-        mate = partner(b)
-        count = lanes >> (b + 1)
-        for i in range(count):
-            turn = (mate // (1 << (b + 1)) + i) % count
-            lane_of = mate % (1 << (b + 1)) + turn * (1 << (b + 1))
-            act_z(b, lane_of).wait_recv()
-            for lower in reversed(range(b)):
-                act_z(lower, lane_of).start()
-            act_out(lane_of)
-
-    for m in range(2):
-        for d in range(lanes):
-            sized(lane, lambda size, m=m, d=d: w_y(m, lane_at(d), other_side, size).wait_recv())
+    for e in range(1, lanes - 1):
+        act_arrived(e)
+    send_weight(1, lanes - 1)
+    share_weight(2)
+    forward_weight(1, mate(1))
 
     few_here = rank(lane) // (lanes - 1)
     unit = lax.broadcasted_iota(jnp.int32, (nt * chunk, width), 1)
@@ -709,23 +746,41 @@
         def _():
             dw[:, last * LANE :, :] = jnp.zeros((n, width - last * LANE, dw.shape[2]), dw.dtype)
 
+    def depth(ref):
+        return ref[...].reshape(ref.shape[0] * ref.shape[1], ref.shape[2])
+
+    for d in range(lanes):
+        w_shared(0, lane_at(d))
+
     @pl.loop(0, lanes)
     def _(i):
-        lane_of = 0
-        for b in range(bits):
-            lane_of = lane_of + (bit_of(lane, b) + bit_of(i, bits - 1 - b)) % 2 * (1 << b)
-
-        @pl.when(i > 0)
-        def _():
-            act_from_x(lane_of)
+        lane_of = mated(i)
+        for e in range(1, lanes):
+
+            @pl.when(i == e)
+            def _(e=e):
+                if e == lanes - 2:
+                    act_arrived(e + 1)
+                    for f in range(1, lanes):
+                        send_weight(2, f)
+                act_from_x(mate(e))
+                if e > 1:
+                    forward_weight(1, mate(e))
 
         for x_of in range(xs):
             act_core(lane_of, x_of, other_core).wait_recv()
         inputs = act[lane_of].reshape(nt * chunk, act.shape[-1])
-        gated = jnp.dot(inputs, gw[...].reshape(n * gw.shape[1], width), preferred_element_type=jnp.float32)
-        lifted = jnp.dot(inputs, uw[...].reshape(n * uw.shape[1], width), preferred_element_type=jnp.float32)
-        hidden = gated * lax.logistic(gated) * lifted
-        hidden = jnp.where(mine, hidden, 0.0).astype(jnp.bfloat16)
+        gated[lane_of] = jnp.dot(inputs, depth(gw), preferred_element_type=jnp.float32)
+
+    for d in range(lanes):
+        w_shared(1, lane_at(d))
+
+    @pl.loop(0, lanes)
+    def _(lane_of):
+        inputs = act[lane_of].reshape(nt * chunk, act.shape[-1])
+        lifted = jnp.dot(inputs, depth(uw), preferred_element_type=jnp.float32)
+        gates = gated[lane_of]
+        hidden = jnp.where(mine, gates * lax.logistic(gates) * lifted, 0.0).astype(jnp.bfloat16)
         for x_of in range(xs):
             for core_of in range(2):
                 start = (x_of * 2 + core_of) * chunk
@@ -759,25 +814,33 @@
         piece = out.at[slot, :, columns(s)]
         return remote(piece, piece, ag_cs.at[s, x_of], ag_r.at[s, slot], at_tp(xi, other_core))
 
+    def lane_in_order(j):
+        return lanes // 2 + (1 - 2 * (j % 2)) * (j // 2) - j % 2
+
     def slot_of(k):
-        j = k // SIDES
-        lane_of = lanes // 2 + (1 - 2 * (j % 2)) * (j // 2) - j % 2
-        return lane_of * SIDES + (side + k) % SIDES
+        return lane_in_order(k % lanes) * SIDES + (side + k // lanes) % SIDES
+
+    upper = lane // (lanes // 2)
+    own_turn = upper * (2 * lane - lanes) + (1 - upper) * (lanes - 1 - 2 * lane)
+
+    def early_slot(k):
+        own = (n - 1 - k) // (n - SIDES)
+        p = (k - SIDES) % (lanes - 1) + 1
+        lane_of = lane_in_order(p - 1 + (p - own_turn + lanes - 1) // lanes)
+        side_of = (1 - own) * ((k - SIDES) // (lanes - 1)) + own * k
+        return (own * lane + (1 - own) * lane_of) * SIDES + (side + side_of) % SIDES
 
     def multiply(k):
-        s = slot_of(k)
-        lane_of, side_of = s // SIDES, s % SIDES
-
-        @pl.when(side_of == side)
+        s = early_slot(k)
+        lane_of = s // SIDES
+
+        @pl.when((k > 1) & (k <= lanes))
         def _():
-            @pl.when(lane_of != lane)
-            def _():
-                w_arrived(2, s)
-                w_forward(2, lane_of)
-
-        @pl.when(side_of != side)
+            forward_weight(2, lane_of)
+
+        @pl.when((k == 1) | (k > lanes))
         def _():
-            sized(lane, lambda size: w_y(2, lane_of, other_side, size).wait_recv())
+            w_shared(2, lane_of)
 
         away = hid[other_core].reshape(share, width)
         core_out[s] = (
@@ -790,7 +853,7 @@
         keep[s] = jnp.dot(near, dw[s], preferred_element_type=jnp.float32).reshape(xs, lanes, chunk, cols)
 
     def reduce_core(k):
-        s = slot_of(k)
+        s = early_slot(k)
         rs_core(s).wait_recv()
         for d in range(1, xs):
             x_to = x_at(d)
@@ -836,19 +899,20 @@
             ag_core(s, x_of, core).start()
 
     stages = [(0, multiply), (1, reduce_core)]
-    at = 3
+    at = 5
     for b in range(bits + 1):
         stages.append((at, functools.partial(reduce_lanes, b)))
         at += 2
-    stages.append((at, spread))
-
-    @pl.loop(0, n + at)
+
+    @pl.loop(0, n + at - 2)
     def _(k):
         for lag, action in reversed(stages):
 
             @pl.when((k >= lag) & (k < n + lag))
             def _(lag=lag, action=action):
                 action(k - lag)
+
+    pl.loop(0, n)(spread)
 
     @pl.loop(0, n)
     def _(s):
@@ -863,9 +927,9 @@
             rs_z(s, b).wait_send()
 
     for d in range(1, lanes):
-        kv_z(d, sp).wait_send()
+        kv_z(d, lane).wait_send()
         for m in range(3):
-            lane_to = lane_at(d)
+            lane_to = mate(d)
             sized(lane_to, lambda size, m=m, d=d, lane_to=lane_to: w_z(m, d, sp, lane_to, size).wait_send())
     for lane_of in range(lanes):
         kv_y(lane_of, side).wait_send()
@@ -877,7 +941,8 @@
             act_core(lane_of, x_of, core).wait_send()
     for b in range(bits):
         for h in range(lanes >> (b + 1)):
-            act_z(b, lane % (1 << (b + 1)) + h * (1 << (b + 1))).wait_send()
+            lane_of = lane % (1 << (b + 1)) + h * (1 << (b + 1))
+            act_z(b, lane_of).wait_send()
     for p in range(PIECES):
         part_core(p).wait_send()
         for d in range(1, xs):
@@ -902,6 +967,12 @@
     span = width // PIECES
     bf, f32 = jnp.bfloat16, jnp.float32
     shapes = [
+        ((rows, heads * head_dim), bf),
+        ((head_dim, rows), bf),
+        ((1, rows), jnp.int32),
+        ((1, head_dim), f32),
+        ((1, head_dim), f32),
+        ((1, width), f32),
         ((n, 2 * head_dim + 16, rows), bf),
         ((heads * head_dim, rows), bf),
         ((heads, 1, rows), f32),
@@ -918,6 +989,7 @@
         ((n, cols, wu), bf),
         ((n, cols, wu), bf),
         ((n, wu, cols), bf),
+        ((lanes, rows, wu), f32),
         ((2, xs, lanes, chunk, wu), bf),
         ((n, xs, lanes, chunk, cols), f32),
         ((n, xs, lanes, chunk, cols), bf),
@@ -937,7 +1009,7 @@
         size += count * jnp.dtype(kind).itemsize
     if size > VMEM_LIMIT * 3 // 4:
         return None
-    sems = [(lanes,), (lanes,), (n,), (3,), (3, lanes), (3, lanes), (3, n), (2,)]
+    sems = [(lanes,), (lanes,), (n,), (3,), (3, lanes), (3, lanes), (3, n), (9,)]
     sems += [(PIECES,), (PIECES,), (PIECES, xs), (PIECES, xs)]
     sems += [(bits, lanes), (xs, lanes), (lanes, xs), (lanes, nt)]
     sems += [(n,), (n,), (n, xs), (n, xs), (n, bits), (n, bits), (n, xs), (n, xs), (n, nt)]
@@ -957,13 +1029,12 @@
     angles = [
         freqs[:, None] * spot.astype(jnp.float32)[None, :] for spot in (places // GRID, places % GRID)
     ]
-    consts = [f(a) for a in angles for f in (jnp.cos, jnp.sin)]
-    consts += [jnp.broadcast_to(g[:, None], (head_dim, rows)) for g in (query_gain, key_norm_scale)]
+    table = jnp.concatenate([f(a) for a in angles for f in (jnp.cos, jnp.sin)], axis=0)
     hbm = pl.BlockSpec(memory_space=pl.ANY)
     out = pl.pallas_call(
         functools.partial(fused_kernel, n, nt, wide),
         out_shape=jax.ShapeDtypeStruct((nt, rows // nt, width), jnp.bfloat16),
-        in_specs=[VM] * 6 + [hbm] * 5,
+        in_specs=[hbm] * 12 + [VM],
         out_specs=VM,
         scratch_shapes=scratch,
         compiler_params=pltpu.CompilerParams(
@@ -971,8 +1042,9 @@
         ),
         name="fused_layer",
     )(
-        queries, keys.T, values.T, doc_ids.reshape(1, rows), jnp.concatenate(consts, axis=0),
-        norm_gain.reshape(1, width), tokens_in, out_weight, gate_weight, up_weight, down_weight,
+        queries, keys.T, values.T, doc_ids.reshape(1, rows), query_gain.reshape(1, head_dim),
+        key_norm_scale.reshape(1, head_dim), norm_gain.reshape(1, width), tokens_in, out_weight,
+        gate_weight, up_weight, down_weight, table,
     )
     return out.reshape(rows, width)
 

time: 132 us -> 116 us (0.88)
  Pallas kernels: 127 us -> 112 us
  local copies, waits for them, and re-layouts: 4.22 us -> 2.3 us
    pallas_call x1, Pallas kernels: 127 us -> 112 us  [fused_layer(): pl.pallas_call(functools.partial(fused_kernel, n, nt, wide), out_shape=ja...]
    unnamed x8 -> x1, local copies, waits for them, and re-layouts: 4.15 us -> 2.3 us
where the time goes in v3:
time: 116 us; the launch traced here: 115 us
  Pallas kernels  112 us (97%)
  local copies, waits for them, and re-layouts  2.3 us (2%)
    pallas_call x1, Pallas kernels, fused_layer(): pl.pallas_call(functools.partial(fused_kernel, n, nt, wide), out_shape=ja...  112 us

profile of v3, /device:TPU:0, one launch (start us, length us, event | category | flops | bytes accessed | tf_op | source)
XLA Modules:
  0.0 115.4 jit_solution(5717812133579534745)
XLA Ops:
  0.0 0.2 multiply_cosine_fusion.1
  0.2 0.6 pad_maximum_fusion.table_ref
  0.9 112.3 %fused_layer.1 = bf16[4,64,2048]{2,1,0:T(8,128)(2,1)} custom-call(bf16[256,256]{1,0:T(8,128)(2,1)} %q_in.1, bf16[64,256]{1,0:T(8,128)(2,1)} %bitcast.8, bf16[64,256]{1,0:T(8,128)(2,1)} %bitcast.9, s32[1,256]{1,0:T(1,128)} %bitcast.11, f32[1,64]{1,0:T(1,128)} %bitcast.12, f32[1,64]{1,0:T(1,128)} %bitcast.13, f32[1,2048]{1,0:T(1,128)} %bitcast.10, ...), custom_call_target="tpu_custom_call" | custom-call | tf_op jit(solution)/shard_map/fused_layer/pallas_call | solution.py:1034
  113.1 2.3 %copy.14 = bf16[256,2048]{1,0:T(8,128)(2,1)} copy(bf16[256,2048]{1,0:T(8,128)(2,1)} %bitcast.7) | data formatting | bytes 2097152
  (2 shorter events, 0.0 us)

commit v4 on v3

--- a/solution.py
+++ b/solution.py
@@ -270,6 +270,7 @@
 SIDES = 2
 LANE = 128
 PIECES = 4
+GATHERED = 2
 
 
 def turned(block, gain, table):
@@ -340,6 +341,9 @@
     px_out,
     px_in,
     ow,
+    ow_all,
+    att_out,
+    att,
     tok,
     resid,
     act,
@@ -369,6 +373,11 @@
     pc_r,
     px_s,
     px_r,
+    ow_xs,
+    ow_cs,
+    ow_r,
+    att_s,
+    att_r,
     act_zs,
     act_xs,
     act_cs,
@@ -438,9 +447,10 @@
     for d in range(1, lanes):
         pl.semaphore_signal(barrier, inc=1, device_id=at_sp(lane_at(d), side), device_id_type=MESH)
     pl.semaphore_signal(barrier, inc=1, device_id=at_sp(lane, other_side), device_id_type=MESH)
-    for d in range(1, xs):
-        pl.semaphore_signal(barrier, inc=1, device_id=at_tp(x_at(d), core), device_id_type=MESH)
-    pl.semaphore_signal(barrier, inc=1, device_id=at_tp(xi, other_core), device_id_type=MESH)
+    for d in range(1, nt):
+        pl.semaphore_signal(
+            barrier, inc=1, device_id={"sp": sp, "tp": (tp + d) % nt}, device_id_type=MESH
+        )
 
     def rank(lane_to):
         return lane_to + core * (lanes - 1 - 2 * lane_to)
@@ -505,7 +515,7 @@
     q_doc = doc_ref[...].astype(jnp.float32)
     kv[sp, kv_docs:kv_vals, :] = jnp.broadcast_to(q_doc, (kv_vals - kv_docs, rows)).astype(jnp.bfloat16)
 
-    pl.semaphore_wait(barrier, lanes - 1 + 1 + xs - 1 + 1)
+    pl.semaphore_wait(barrier, lanes - 1 + 1 + nt - 1)
 
     def kv_z(e, lane_of):
         slot = lane_of * SIDES + side
@@ -520,6 +530,23 @@
     for e in range(1, lanes):
         kv_z(e, lane).start()
     kv_y(lane, side).start()
+
+    span = ow.shape[1] // PIECES
+    gathered = GATHERED * span
+    ow_here = out_weight.at[:, 0:gathered]
+
+    def ow_x(d, slot):
+        return remote(ow_here, ow_all.at[slot], ow_xs.at[d], ow_r.at[slot], at_tp(x_at(d), core))
+
+    def ow_core(x_of, core_of):
+        slot = x_of * 2 + core_of
+        return remote(
+            ow_all.at[slot], ow_all.at[slot], ow_cs.at[x_of], ow_r.at[slot], at_tp(xi, other_core)
+        )
+
+    for d in range(1, xs):
+        ow_x(d, tp).start()
+    remote(ow_here, ow_all.at[tp], ow_cs.at[xi], ow_r.at[tp], at_tp(xi, other_core)).start()
 
     def w_z(m, e, slot, lane_to, size):
         return remote(
@@ -634,7 +661,15 @@
         pieces.append((acc[at, :] / total[h]).astype(jnp.bfloat16))
     attended = flipped(jnp.concatenate(pieces, axis=0)).astype(jnp.bfloat16)
 
-    span = ow.shape[1] // PIECES
+    def att_copy(d, peer, slot):
+        return remote(
+            att_out.at[peer], att.at[slot], att_s.at[d], att_r.at[slot], {"sp": sp, "tp": peer}
+        )
+
+    for i in range(nt):
+        att_out[i] = attended[i * chunk : (i + 1) * chunk]
+    for d in range(1, nt):
+        att_copy(d, (tp + d) % nt, tp).start()
 
     def part_core(p):
         return remote(part.at[p, other_core], part_in.at[p], pc_s.at[p], pc_r.at[p], at_tp(xi, other_core))
@@ -643,7 +678,7 @@
         return remote(px_out.at[p, d], px_in.at[p, d], px_s.at[p, d], px_r.at[p, d], at_tp(x_at(d), core))
 
     ow_copy.wait()
-    for p in range(PIECES):
+    for p in range(GATHERED, PIECES):
         product = jnp.dot(
             attended, ow[:, p * span : (p + 1) * span], preferred_element_type=jnp.float32
         ).astype(jnp.bfloat16)
@@ -652,8 +687,19 @@
                 start = (x_of * 2 + core_of) * chunk
                 part[p, core_of, x_of] = product[start : start + chunk]
         part_core(p).start()
+    for d in range(1, xs):
+        x_of = x_at(xs - d)
+        ow_x(d, x_of * 2 + core).wait_recv()
+        ow_core(x_of, core).start()
     tok_copy.wait()
-    for p in range(PIECES):
+    early = slice(0, gathered)
+
+    def project(rows_of, weight):
+        product = jnp.dot(rows_of, weight, preferred_element_type=jnp.float32)
+        return product.astype(jnp.bfloat16).astype(jnp.float32)
+
+    resid[:, early] = tok[:, early].astype(jnp.float32) + project(att_out[tp], ow[:, early])
+    for p in range(GATHERED, PIECES):
         at = slice(p * span, (p + 1) * span)
         part_core(p).wait_recv()
         for d in range(1, xs):
@@ -667,7 +713,19 @@
             + part[p, core, xi].astype(jnp.float32)
             + part_in[p, xi].astype(jnp.float32)
         )
-    for p in range(PIECES):
+
+    def add_rows(slot):
+        att_copy(1, tp, slot).wait_recv()
+        resid[:, early] += project(att[slot], ow_all[slot])
+
+    ow_core(xi, other_core).wait_recv()
+    add_rows(xi * 2 + other_core)
+    for d in range(1, xs):
+        add_rows(x_at(xs - d) * 2 + core)
+    for d in range(1, xs):
+        ow_core(x_at(xs - d), other_core).wait_recv()
+        add_rows(x_at(xs - d) * 2 + other_core)
+    for p in range(GATHERED, PIECES):
         at = slice(p * span, (p + 1) * span)
         for d in range(1, xs):
             part_x(p, d).wait_recv()
@@ -763,9 +821,9 @@
                     act_arrived(e + 1)
                     for f in range(1, lanes):
                         send_weight(2, f)
-                act_from_x(mate(e))
                 if e > 1:
                     forward_weight(1, mate(e))
+                act_from_x(mate(e))
 
         for x_of in range(xs):
             act_core(lane_of, x_of, other_core).wait_recv()
@@ -786,6 +844,8 @@
                 start = (x_of * 2 + core_of) * chunk
                 hid[core_of, x_of, lane_of] = hidden[start : start + chunk]
 
+    forward_weight(2, mate(1))
+
     cols = dw.shape[2]
     share = xs * lanes * chunk
     starts = [lanes - (lanes >> b) for b in range(bits)]
@@ -834,7 +894,7 @@
         s = early_slot(k)
         lane_of = s // SIDES
 
-        @pl.when((k > 1) & (k <= lanes))
+        @pl.when((k > 1) & (k <= lanes) & (lane_of != mate(1)))
         def _():
             forward_weight(2, lane_of)
 
@@ -898,15 +958,14 @@
             ag_x(s, d, x_of * 2 + core).wait_recv()
             ag_core(s, x_of, core).start()
 
+    first, gap = 5, 3
     stages = [(0, multiply), (1, reduce_core)]
-    at = 5
     for b in range(bits + 1):
-        stages.append((at, functools.partial(reduce_lanes, b)))
-        at += 2
-
-    @pl.loop(0, n + at - 2)
+        stages.append((first + gap * b, functools.partial(reduce_lanes, b)))
+
+    @pl.loop(0, n + stages[-1][0])
     def _(k):
-        for lag, action in reversed(stages):
+        for lag, action in [stages[1], stages[0]] + stages[:1:-1]:
 
             @pl.when((k >= lag) & (k < n + lag))
             def _(lag=lag, action=action):
@@ -943,7 +1002,13 @@
         for h in range(lanes >> (b + 1)):
             lane_of = lane % (1 << (b + 1)) + h * (1 << (b + 1))
             act_z(b, lane_of).wait_send()
-    for p in range(PIECES):
+    for d in range(1, xs):
+        ow_x(d, tp).wait_send()
+    for x_of in range(xs):
+        ow_core(x_of, core).wait_send()
+    for d in range(1, nt):
+        att_copy(d, (tp + d) % nt, tp).wait_send()
+    for p in range(GATHERED, PIECES):
         part_core(p).wait_send()
         for d in range(1, xs):
             part_x(p, d).wait_send()
@@ -983,6 +1048,9 @@
         ((PIECES, xs, chunk, span), bf),
         ((PIECES, xs, chunk, span), bf),
         ((heads * head_dim, width), bf),
+        ((nt, heads * head_dim, GATHERED * span), bf),
+        ((nt, chunk, heads * head_dim), bf),
+        ((nt, chunk, heads * head_dim), bf),
         ((chunk, width), bf),
         ((chunk, width), f32),
         ((lanes, nt, chunk, width), bf),
@@ -1010,7 +1078,7 @@
     if size > VMEM_LIMIT * 3 // 4:
         return None
     sems = [(lanes,), (lanes,), (n,), (3,), (3, lanes), (3, lanes), (3, n), (9,)]
-    sems += [(PIECES,), (PIECES,), (PIECES, xs), (PIECES, xs)]
+    sems += [(PIECES,), (PIECES,), (PIECES, xs), (PIECES, xs), (xs,), (xs,), (nt,), (nt,), (nt,)]
     sems += [(bits, lanes), (xs, lanes), (lanes, xs), (lanes, nt)]
     sems += [(n,), (n,), (n, xs), (n, xs), (n, bits), (n, bits), (n, xs), (n, xs), (n, nt)]
     return wide, [pltpu.VMEM(*s) for s in shapes] + [pltpu.SemaphoreType.DMA(s) for s in sems]

time: 116 us -> 111 us (0.957)
  Pallas kernels: 112 us -> 108 us
    pallas_call x1, Pallas kernels: 112 us -> 108 us  [fused_layer(): pl.pallas_call(functools.partial(fused_kernel, n, nt, wide), out_shape=ja...]
where the time goes in v4:
time: 111 us
  Pallas kernels  108 us (97%)
  local copies, waits for them, and re-layouts  2.3 us (2%)
    pallas_call x1, Pallas kernels, fused_layer(): pl.pallas_call(functools.partial(fused_kernel, n, nt, wide), out_shape=ja...  108 us
    unnamed x1, local copies, waits for them, and re-layouts  2.3 us

profile of v4, /device:TPU:0, one launch (start us, length us, event | category | flops | bytes accessed | tf_op | source)
XLA Modules:
  0.0 111.1 jit_solution(2273268045534530537)
XLA Ops:
  0.0 0.2 multiply_cosine_fusion.1
  0.2 0.6 pad_maximum_fusion.table_ref
  0.9 107.9 %fused_layer.1 = bf16[4,64,2048]{2,1,0:T(8,128)(2,1)} custom-call(bf16[256,256]{1,0:T(8,128)(2,1)} %q_in.1, bf16[64,256]{1,0:T(8,128)(2,1)} %bitcast.8, bf16[64,256]{1,0:T(8,128)(2,1)} %bitcast.9, s32[1,256]{1,0:T(1,128)} %bitcast.11, f32[1,64]{1,0:T(1,128)} %bitcast.12, f32[1,64]{1,0:T(1,128)} %bitcast.13, f32[1,2048]{1,0:T(1,128)} %bitcast.10, ...), custom_call_target="tpu_custom_call" | custom-call | tf_op jit(solution)/shard_map/fused_layer/pallas_call | solution.py:1102
  108.8 2.3 %copy.14 = bf16[256,2048]{1,0:T(8,128)(2,1)} copy(bf16[256,2048]{1,0:T(8,128)(2,1)} %bitcast.7) | data formatting | bytes 2097152
  (2 shorter events, 0.0 us)

commit v5 on v4

--- a/solution.py
+++ b/solution.py
@@ -282,8 +282,7 @@
     for part in range(2):
         first = full[part * half : part * half + quarter]
         second = full[part * half + quarter : (part + 1) * half]
-        cosine = table[2 * part * quarter : (2 * part + 1) * quarter]
-        sine = table[(2 * part + 1) * quarter : (2 * part + 2) * quarter]
+        cosine, sine = table[2 * part], table[2 * part + 1]
         pieces += [first * cosine - second * sine, second * cosine + first * sine]
     return jnp.concatenate(pieces, axis=0)
 
@@ -323,75 +322,77 @@
     gate,
     up,
     down,
-    table_ref,
-    out,
-    q_raw,
-    k_raw,
-    doc_ref,
-    q_gain_ref,
-    k_gain_ref,
-    norm_gain,
-    kv,
-    q_ref,
-    top,
-    total,
-    acc,
-    part,
-    part_in,
-    px_out,
-    px_in,
-    ow,
-    ow_all,
-    att_out,
-    att,
-    tok,
-    resid,
-    act,
-    gw,
-    uw,
-    dw,
-    gated,
-    hid,
-    keep,
-    core_out,
-    core_in,
-    x_keep,
-    x_out,
-    x_in,
-    z_keep,
-    z_out,
-    z_in,
-    kv_zs,
-    kv_ys,
-    kv_r,
-    w_own,
-    w_zs,
-    w_ys,
-    w_r,
-    misc,
-    pc_s,
-    pc_r,
-    px_s,
-    px_r,
-    ow_xs,
-    ow_cs,
-    ow_r,
-    att_s,
-    att_r,
-    act_zs,
-    act_xs,
-    act_cs,
-    act_r,
-    rs_cs,
-    rs_cr,
-    rs_xs,
-    rs_xr,
-    rs_zs,
-    rs_zr,
-    ag_xs,
-    ag_cs,
-    ag_r,
+    *rest,
 ):
+    tables, (out, scratch) = rest[:4], (rest[4], rest[5:])
+    (
+        q_raw,
+        k_raw,
+        doc_ref,
+        q_gain_ref,
+        k_gain_ref,
+        norm_gain,
+        kv,
+        q_ref,
+        top,
+        total,
+        acc,
+        part,
+        part_in,
+        px_out,
+        px_in,
+        ow,
+        ow_all,
+        att_out,
+        att,
+        tok,
+        resid,
+        act,
+        gw,
+        uw,
+        dw,
+        gated,
+        hid,
+        keep,
+        core_out,
+        core_in,
+        x_keep,
+        x_out,
+        x_in,
+        z_keep,
+        z_out,
+        z_in,
+        kv_zs,
+        kv_ys,
+        kv_r,
+        w_own,
+        w_zs,
+        w_ys,
+        w_r,
+        misc,
+        pc_s,
+        pc_r,
+        px_s,
+        px_r,
+        ow_xs,
+        ow_cs,
+        ow_r,
+        att_s,
+        att_r,
+        act_zs,
+        act_xs,
+        act_cs,
+        act_r,
+        rs_cs,
+        rs_cr,
+        rs_xs,
+        rs_xr,
+        rs_zs,
+        rs_zr,
+        ag_xs,
+        ag_cs,
+        ag_r,
+    ) = scratch
     sp, tp = lax.axis_index("sp"), lax.axis_index("tp")
     lanes, xs = n // SIDES, nt // 2
     bits = lanes.bit_length() - 1
@@ -405,7 +406,7 @@
     width = wide * LANE
     last = blocks - (lanes - 1) * wide
     kv_docs = head_dim
-    table = table_ref[...]
+    table = tuple(ref[...] for ref in tables)
 
     def at_sp(lane_to, side_to):
         return {"sp": lane_to * SIDES + side_to, "tp": tp}
@@ -844,7 +845,8 @@
                 start = (x_of * 2 + core_of) * chunk
                 hid[core_of, x_of, lane_of] = hidden[start : start + chunk]
 
-    forward_weight(2, mate(1))
+    for e in range(1, lanes // 2):
+        forward_weight(2, mate(e))
 
     cols = dw.shape[2]
     share = xs * lanes * chunk
@@ -874,33 +876,29 @@
         piece = out.at[slot, :, columns(s)]
         return remote(piece, piece, ag_cs.at[s, x_of], ag_r.at[s, slot], at_tp(xi, other_core))
 
-    def lane_in_order(j):
-        return lanes // 2 + (1 - 2 * (j % 2)) * (j // 2) - j % 2
-
-    def slot_of(k):
-        return lane_in_order(k % lanes) * SIDES + (side + k // lanes) % SIDES
-
-    upper = lane // (lanes // 2)
-    own_turn = upper * (2 * lane - lanes) + (1 - upper) * (lanes - 1 - 2 * lane)
-
-    def early_slot(k):
-        own = (n - 1 - k) // (n - SIDES)
-        p = (k - SIDES) % (lanes - 1) + 1
-        lane_of = lane_in_order(p - 1 + (p - own_turn + lanes - 1) // lanes)
-        side_of = (1 - own) * ((k - SIDES) // (lanes - 1)) + own * k
-        return (own * lane + (1 - own) * lane_of) * SIDES + (side + side_of) % SIDES
+    half = lanes // 2
+    upper = lane // half
+
+    def half_slot(k):
+        turn = k % lanes
+        lane_of = (upper + k // lanes) % 2 * half + turn % half
+        return lane_of * SIDES + (side + turn // half) % SIDES
+
+    def slot_of(i):
+        turn = i // 2
+        lane_of = i % 2 * half + turn % half
+        return lane_of * SIDES + (side + turn // half) % SIDES
 
     def multiply(k):
-        s = early_slot(k)
-        lane_of = s // SIDES
-
-        @pl.when((k > 1) & (k <= lanes) & (lane_of != mate(1)))
+        s = half_slot(k)
+
+        @pl.when((k >= lanes - 1) & (k < lanes - 1 + half))
         def _():
-            forward_weight(2, lane_of)
-
-        @pl.when((k == 1) | (k > lanes))
+            forward_weight(2, (upper + 1) % 2 * half + k - (lanes - 1))
+
+        @pl.when(k % lanes >= half)
         def _():
-            w_shared(2, lane_of)
+            w_shared(2, s // SIDES)
 
         away = hid[other_core].reshape(share, width)
         core_out[s] = (
@@ -913,7 +911,7 @@
         keep[s] = jnp.dot(near, dw[s], preferred_element_type=jnp.float32).reshape(xs, lanes, chunk, cols)
 
     def reduce_core(k):
-        s = early_slot(k)
+        s = half_slot(k)
         rs_core(s).wait_recv()
         for d in range(1, xs):
             x_to = x_at(d)
@@ -922,7 +920,7 @@
         x_keep[s] = keep[s, xi] + core_in[s, xi].astype(jnp.float32)
 
     def reduce_lanes(b, k):
-        s = slot_of(k)
+        s = half_slot(k) if b < bits - 1 else slot_of(k)
         if b == 0:
             for d in range(1, xs):
                 rs_x(s, d).wait_recv()
@@ -958,16 +956,28 @@
             ag_x(s, d, x_of * 2 + core).wait_recv()
             ag_core(s, x_of, core).start()
 
-    first, gap = 5, 3
-    stages = [(0, multiply), (1, reduce_core)]
-    for b in range(bits + 1):
-        stages.append((first + gap * b, functools.partial(reduce_lanes, b)))
-
-    @pl.loop(0, n + stages[-1][0])
+    def by_two(b):
+        def both(j):
+            for i in range(2):
+                reduce_lanes(b, 2 * j + i)
+
+        return both
+
+    lag = 4
+    stages = [(0, n, multiply), (1, n, reduce_core)]
+    for b in range(bits - 1):
+        stages.append((lag, n, functools.partial(reduce_lanes, b)))
+        lag += 2
+    lag += lanes - 1 if bits > 1 else lanes
+    for b in (bits - 1, bits):
+        stages.append((lag, n // 2, by_two(b)))
+        lag += 2
+
+    @pl.loop(0, stages[-1][0] + n // 2)
     def _(k):
-        for lag, action in [stages[1], stages[0]] + stages[:1:-1]:
-
-            @pl.when((k >= lag) & (k < n + lag))
+        for lag, count, action in [stages[1], stages[0]] + stages[2:]:
+
+            @pl.when((k >= lag) & (k < count + lag))
             def _(lag=lag, action=action):
                 action(k - lag)
 
@@ -1097,12 +1107,12 @@
     angles = [
         freqs[:, None] * spot.astype(jnp.float32)[None, :] for spot in (places // GRID, places % GRID)
     ]
-    table = jnp.concatenate([f(a) for a in angles for f in (jnp.cos, jnp.sin)], axis=0)
+    tables = [f(a) for a in angles for f in (jnp.cos, jnp.sin)]
     hbm = pl.BlockSpec(memory_space=pl.ANY)
     out = pl.pallas_call(
         functools.partial(fused_kernel, n, nt, wide),
         out_shape=jax.ShapeDtypeStruct((nt, rows // nt, width), jnp.bfloat16),
-        in_specs=[hbm] * 12 + [VM],
+        in_specs=[hbm] * 12 + [VM] * 4,
         out_specs=VM,
         scratch_shapes=scratch,
         compiler_params=pltpu.CompilerParams(
@@ -1112,7 +1122,7 @@
     )(
         queries, keys.T, values.T, doc_ids.reshape(1, rows), query_gain.reshape(1, head_dim),
         key_norm_scale.reshape(1, head_dim), norm_gain.reshape(1, width), tokens_in, out_weight,
-        gate_weight, up_weight, down_weight, table,
+        gate_weight, up_weight, down_weight, *tables,
     )
     return out.reshape(rows, width)
 

time: 111 us -> 110 us (level)
  Pallas kernels: 108 us -> 106 us
    pallas_call x1, Pallas kernels: 108 us -> 106 us  [fused_layer(): pl.pallas_call(functools.partial(fused_kernel, n, nt, wide), out_shape=ja...]
where the time goes in v5:
time: 110 us
  Pallas kernels  106 us (96%)
  local copies, waits for them, and re-layouts  2.3 us (2%)
    pallas_call x1, Pallas kernels, fused_layer(): pl.pallas_call(functools.partial(fused_kernel, n, nt, wide), out_shape=ja...  106 us
    unnamed x1, local copies, waits for them, and re-layouts  2.3 us

profile of v5, /device:TPU:0, one launch (start us, length us, event | category | flops | bytes accessed | tf_op | source)
XLA Modules:
  0.0 109.6 jit_solution(672133808703359174)
XLA Ops:
  0.0 0.8 multiply_sine_fusion
  0.8 106.4 %fused_layer.1 = bf16[4,64,2048]{2,1,0:T(8,128)(2,1)} custom-call(bf16[256,256]{1,0:T(8,128)(2,1)} %q_in.1, bf16[64,256]{1,0:T(8,128)(2,1)} %bitcast.8, bf16[64,256]{1,0:T(8,128)(2,1)} %bitcast.9, s32[1,256]{1,0:T(1,128)} %bitcast.11, f32[1,64]{1,0:T(1,128)} %bitcast.12, f32[1,64]{1,0:T(1,128)} %bitcast.13, f32[1,2048]{1,0:T(1,128)} %bitcast.10, ...), custom_call_target="tpu_custom_call" | custom-call | tf_op jit(solution)/shard_map/fused_layer/pallas_call | solution.py:1112
  107.3 2.3 %copy.14 = bf16[256,2048]{1,0:T(8,128)(2,1)} copy(bf16[256,2048]{1,0:T(8,128)(2,1)} %bitcast.7) | data formatting | bytes 2097152
  (2 shorter events, 0.0 us)

commit v6 on v5

--- a/solution.py
+++ b/solution.py
@@ -975,7 +975,7 @@
 
     @pl.loop(0, stages[-1][0] + n // 2)
     def _(k):
-        for lag, count, action in [stages[1], stages[0]] + stages[2:]:
+        for lag, count, action in stages:
 
             @pl.when((k >= lag) & (k < count + lag))
             def _(lag=lag, action=action):

time: 110 us -> 110 us (level)
  no operation moved by 1% of the time
where the time goes in v6:
time: 110 us
  Pallas kernels  107 us (97%)
  local copies, waits for them, and re-layouts  2.3 us (2%)
    pallas_call x1, Pallas kernels, fused_layer(): pl.pallas_call(functools.partial(fused_kernel, n, nt, wide), out_shape=ja...  107 us
    unnamed x1, local copies, waits for them, and re-layouts  2.3 us

profile of v6, /device:TPU:0, one launch (start us, length us, event | category | flops | bytes accessed | tf_op | source)
XLA Modules:
  0.0 109.9 jit_solution(5603121867212925546)
XLA Ops:
  0.0 0.8 multiply_sine_fusion
  0.8 106.8 %fused_layer.1 = bf16[4,64,2048]{2,1,0:T(8,128)(2,1)} custom-call(bf16[256,256]{1,0:T(8,128)(2,1)} %q_in.1, bf16[64,256]{1,0:T(8,128)(2,1)} %bitcast.8, bf16[64,256]{1,0:T(8,128)(2,1)} %bitcast.9, s32[1,256]{1,0:T(1,128)} %bitcast.11, f32[1,64]{1,0:T(1,128)} %bitcast.12, f32[1,64]{1,0:T(1,128)} %bitcast.13, f32[1,2048]{1,0:T(1,128)} %bitcast.10, ...), custom_call_target="tpu_custom_call" | custom-call | tf_op jit(solution)/shard_map/fused_layer/pallas_call | solution.py:1112
  107.6 2.3 %copy.14 = bf16[256,2048]{1,0:T(8,128)(2,1)} copy(bf16[256,2048]{1,0:T(8,128)(2,1)} %bitcast.7) | data formatting | bytes 2097152
  (2 shorter events, 0.0 us)
